TPU v7x, 512 devices: a whole 4x4x16 slice. The times are simulated.
512 devices in a mesh: sp: 64 (over z, y), tp: 8 (over x, core).
Axes of the slice: x: 4, y: 4, z: 16, core: 2. Of those that a mesh axis runs over, the one named last changes fastest.
Arguments:
- activations: bfloat16 [16384, 2048], P('sp', 'tp'), may hold values from -8 to 8
- norm_gain: float32 [2048], replicated, may hold values from 0.1 to 1.9
- win_query: bfloat16 [2048, 1024], P(None, 'tp'), may hold values from -1 to 1
- win_key: bfloat16 [2048, 512], P(None, 'tp'), may hold values from -1 to 1
- win_value: bfloat16 [2048, 512], P(None, 'tp'), may hold values from -0.125 to 0.125
- sink_logit: float32 [16], P('tp'), may hold values from 1 to 6
- lat_query: bfloat16 [2048, 1536], P(None, 'tp'), may hold values from -1 to 1
- key_value_down_weight: bfloat16 [2048, 128], replicated, may hold values from -0.125 to 0.125
- rope_key: bfloat16 [2048, 64], replicated, may hold values from -1 to 1
- latent_norm_gain: float32 [128], replicated, may hold values from 0.1 to 1.9
- key_up_weight: bfloat16 [128, 1024], P(None, 'tp'), may hold values from -0.5 to 0.5
- value_up_weight: bfloat16 [128, 1024], P(None, 'tp'), may hold values from -0.5 to 0.5
- out_win: bfloat16 [1024, 2048], P('tp'), may hold values from -0.359375 to 0.359375
- out_lat: bfloat16 [1024, 2048], P('tp'), may hold values from -0.59765625 to 0.59765625
Outputs:
- mixed: bfloat16 [16384, 2048], P('sp', 'tp')
All inputs are finite; a program needn't handle non-finite values.
Results may differ from a plain program's by a relative error of at most 0.025.
Values may be sent and summed in bfloat16 or wider, within the bound.
A program may use at most 64 MiB of HBM per device.

v0:
```python
from functools import partial

import jax
import jax.numpy as jnp
from jax import lax
from jax.sharding import PartitionSpec as P

HEADS_A = 16
DH = 64
WINDOW = 128
UNROTATED_WIDTH = 128
D_ROPE = 64
VALUE_WIDTH = 128


EPSILON = 1e-06
ROPE_BASE = 10000.0


def in_order(tiles, dim):
    dims = list(tiles.shape[1:])
    dims[dim] *= tiles.shape[0]
    return jnp.moveaxis(tiles, 0, dim).reshape(dims)


def from_everyone(x, axis):
    copies = jnp.broadcast_to(x, (lax.axis_size(axis), *x.shape))
    return lax.all_to_all(copies, axis, split_axis=0, concat_axis=0, tiled=True)


def gather_directly(x, axis, dim):
    return in_order(from_everyone(x, axis), dim)


def padded_2(cells, sides, width):
    for axis, dim in sides:
        count = lax.axis_size(axis)
        ends = count - 1
        head = lax.slice_in_dim(cells, 0, width, axis=dim)
        tail = lax.slice_in_dim(cells, cells.shape[dim] - width, cells.shape[dim], axis=dim)
        cells = jnp.concatenate(
            [
                lax.ppermute(tail, axis, [(i, (i + 1) % count) for i in range(ends)]),
                cells,
                lax.ppermute(head, axis, [((i + 1) % count, i) for i in range(ends)]),
            ],
            axis=dim,
        )
    return cells


def in_one_piece(arrays, axis, dim, along):
    widths = [a.shape[along] for a in arrays]
    both = jnp.concatenate(arrays, axis=along)
    whole = lax.all_gather(both, axis, axis=dim, tiled=True)
    return tuple(jnp.split(whole, [sum(widths[:k]) for k in range(1, len(widths))], axis=along))


def sent_together(arrays, axis, split_dim, concat_dim, along):
    columns = [a.reshape(*a.shape[:along], -1) for a in arrays]
    both = jnp.concatenate(columns, axis=along)
    whole, at, finished = (
        lax.all_to_all(both, axis, split_axis=split_dim, concat_axis=concat_dim, tiled=True),
        0,
        [],
    )
    for a, column in zip(arrays, columns):
        piece = whole[..., at : at + column.shape[along]]
        finished.append(piece.reshape(*piece.shape[:along], *a.shape[along:]))
        at += column.shape[along]
    return tuple(finished)


def in_blocks(x, dim, count):
    dims = x.shape
    tiles = x.reshape(*dims[:dim], count, dims[dim] // count, *dims[dim + 1 :])
    return jnp.moveaxis(tiles, dim, 0)


def sent_and_summed(x, axis, dim):
    tiles = in_blocks(x, dim, lax.axis_size(axis))
    arrived = lax.all_to_all(tiles, axis, split_axis=0, concat_axis=0, tiled=True)
    return arrived.astype(jnp.float32).sum(axis=0)


def rotate(vectors, angles):
    half_width = vectors.shape[-1] // 2
    cosine_table = jnp.cos(angles)
    sine_table = jnp.sin(angles)
    lower_half = vectors[..., :half_width]
    upper_half = vectors[..., half_width:]
    return jnp.concatenate(
        [
            lower_half * cosine_table - upper_half * sine_table,
            lower_half * sine_table + upper_half * cosine_table,
        ],
        axis=-1,
    )


def rotary_angles(places, width):
    frequency = 1.0 / ROPE_BASE ** (jnp.arange(0, width, 2).astype(jnp.float32) / width)
    return places[:, None] * frequency[None, :]


def window_attention(queries, padded, sinks, offset, seq_total, head_start):
    tok_rows = queries.shape[0]
    key_heads = padded.shape[1] // (2 * DH)
    groups = queries.shape[1] // (DH * key_heads)
    key_rows = padded[:, : key_heads * DH].reshape(-1, key_heads, DH)
    value_rows = padded[:, key_heads * DH :].reshape(-1, key_heads, DH)
    grouped = queries.reshape(tok_rows, key_heads, groups, DH)
    scores = jnp.einsum(
        "qhgd,khd->hgqk", grouped, key_rows, preferred_element_type=jnp.float32
    ) * DH ** (-0.5)
    query_pos = offset + jnp.arange(tok_rows, dtype=jnp.int32)
    key_pos = offset - WINDOW + jnp.arange(tok_rows + 2 * WINDOW, dtype=jnp.int32)
    distance = jnp.abs(query_pos[:, None] - key_pos[None, :])
    in_window = (distance <= WINDOW) & (key_pos[None, :] >= 0) & (key_pos[None, :] < seq_total)
    head_ids = head_start + jnp.arange(key_heads * groups, dtype=jnp.int32)
    slopes = jnp.exp2(-8.0 * (head_ids + 1).astype(jnp.float32) / HEADS_A).reshape(
        key_heads, groups
    )
    scores = scores - slopes[:, :, None, None] * distance.astype(jnp.float32)[None, None]
    scores = jnp.where(in_window[None, None], scores, -jnp.inf)
    sink_table = sinks.reshape(key_heads, groups)
    row_peak = jnp.maximum(jnp.max(scores, axis=3), sink_table[:, :, None])
    weights = jnp.exp(scores - row_peak[..., None])
    denominator = jnp.sum(weights, axis=3) + jnp.exp(sink_table[:, :, None] - row_peak)
    blended = jnp.einsum(
        "hgqk,khd->qhgd",
        weights.astype(jnp.bfloat16),
        value_rows,
        preferred_element_type=jnp.float32,
    )
    blended = blended / jnp.transpose(denominator, (2, 0, 1))[..., None]
    return blended.reshape(tok_rows, key_heads * groups * DH).astype(jnp.bfloat16)


def latent_step(running, key_block, query_plain, query_turned):
    row_peak, totals, weighted = running
    keys_plain, values_plain, keys_turned = key_block
    key_count = keys_plain.shape[0]
    head_count = query_plain.shape[1]
    scores = jnp.einsum(
        "qhd,khd->hqk",
        query_plain,
        keys_plain.reshape(key_count, head_count, UNROTATED_WIDTH),
        preferred_element_type=jnp.float32,
    )
    scores = scores + jnp.einsum(
        "qhd,kd->hqk", query_turned, keys_turned, preferred_element_type=jnp.float32
    )
    scores = scores * (UNROTATED_WIDTH + D_ROPE) ** (-0.5)
    new_peak = jnp.maximum(row_peak, jnp.max(scores, axis=2))
    factor = jnp.exp(row_peak - new_peak)
    weights = jnp.exp(scores - new_peak[..., None])
    totals = totals * factor + jnp.sum(weights, axis=2)
    weighted = weighted * factor[..., None] + jnp.einsum(
        "hqk,khd->hqd",
        weights.astype(jnp.bfloat16),
        values_plain.reshape(key_count, head_count, VALUE_WIDTH),
        preferred_element_type=jnp.float32,
    )
    return (new_peak, totals, weighted)


def over_blocks(running, pieces, prepare, attend, block_rows):
    key_count = pieces[0].shape[0]
    stacked = tuple(
        (
            piece_part.reshape((key_count // block_rows, block_rows) + piece_part.shape[1:])
            for piece_part in pieces
        )
    )

    def one_block(state_now, key_block):
        return (attend(state_now, prepare(key_block)), None)

    return lax.scan(one_block, running, stacked)[0]


def per_device(
    activations,
    norm_gain,
    win_query,
    win_key,
    win_value,
    sink_logit,
    lat_query,
    key_value_down_weight,
    rope_key,
    latent_norm_gain,
    key_up_weight,
    value_up_weight,
    out_win,
    out_lat,
):
    tok_rows = activations.shape[0]
    weights_all = (win_query, win_key, win_value, lat_query, key_value_down_weight, rope_key)
    widened = gather_directly(activations, "tp", 1).astype(jnp.float32)
    normalized = (widened * norm_gain[None, :]).astype(jnp.bfloat16)
    squares = jnp.sum(widened * widened, axis=1)
    totals = tuple(
        (jnp.dot(normalized, weight, preferred_element_type=jnp.float32) for weight in weights_all)
    )
    squares, totals = (squares, totals)
    win_proj, key_proj, value_proj, latq_proj, compressed, rope_proj = totals
    row_scale = lax.rsqrt(squares / norm_gain.shape[0] + EPSILON)[:, None]
    offset = lax.axis_index("sp") * tok_rows
    seq_total = tok_rows * lax.axis_size("sp")
    places = (offset + jnp.arange(tok_rows, dtype=jnp.int32)).astype(jnp.float32)
    angles = rotary_angles(places, D_ROPE)
    win_queries = (win_proj * row_scale).astype(jnp.bfloat16)
    key_value = jnp.concatenate(
        [
            (key_proj * row_scale).astype(jnp.bfloat16),
            (value_proj * row_scale).astype(jnp.bfloat16),
        ],
        axis=1,
    )
    padded = padded_2(key_value, (("sp", 0),), WINDOW)
    head_start = lax.axis_index("tp") * sink_logit.shape[0]
    win_out = window_attention(win_queries, padded, sink_logit, offset, seq_total, head_start)
    head_count = lat_query.shape[1] // (UNROTATED_WIDTH + D_ROPE)
    query_all = (latq_proj * row_scale).reshape(tok_rows, head_count, UNROTATED_WIDTH + D_ROPE)
    query_plain = query_all[..., :UNROTATED_WIDTH].astype(jnp.bfloat16)
    query_turned = rotate(query_all[..., UNROTATED_WIDTH:], angles[:, None, :]).astype(jnp.bfloat16)
    latent = (
        compressed
        * lax.rsqrt(jnp.mean(compressed * compressed, axis=1, keepdims=True) + EPSILON)
        * latent_norm_gain[None, :]
    ).astype(jnp.bfloat16)
    key_rotary = rotate(rope_proj * row_scale, angles).astype(jnp.bfloat16)
    tp_count = lax.axis_size("tp")
    every_plain, every_turned = in_one_piece((query_plain, query_turned), "tp", 1, 2)
    key_up_all, value_up_all = in_one_piece((key_up_weight, value_up_weight), "tp", 1, 0)
    all_heads = every_plain.shape[1]
    slice_rows = tok_rows // tp_count
    slice_start = lax.axis_index("tp") * slice_rows
    latent_slice = lax.dynamic_slice_in_dim(latent, slice_start, slice_rows, 0)
    rotary_slice = lax.dynamic_slice_in_dim(key_rotary, slice_start, slice_rows, 0)
    attend_all = partial(latent_step, query_plain=every_plain, query_turned=every_turned)

    def expand_all(key_block):
        return (
            jnp.dot(key_block[0], key_up_all, preferred_element_type=jnp.float32).astype(
                jnp.bfloat16
            ),
            jnp.dot(key_block[0], value_up_all, preferred_element_type=jnp.float32).astype(
                jnp.bfloat16
            ),
            key_block[1],
        )

    part_peak, part_totals, part_weighted = over_blocks(
        (
            jnp.full((all_heads, tok_rows), -jnp.inf, jnp.float32),
            jnp.zeros((all_heads, tok_rows), jnp.float32),
            jnp.zeros((all_heads, tok_rows, VALUE_WIDTH), jnp.float32),
        ),
        in_one_piece((latent_slice, rotary_slice), "sp", 0, 1),
        expand_all,
        attend_all,
        256,
    )
    got_peak, got_totals, got_weighted = tuple(
        (
            part.astype(jnp.float32)
            for part in sent_together(
                (
                    part_peak[None].astype(jnp.bfloat16),
                    part_totals[None].astype(jnp.bfloat16),
                    part_weighted[None].astype(jnp.bfloat16),
                ),
                "tp",
                1,
                0,
                3,
            )
        )
    )
    row_peak = jnp.max(got_peak, axis=0)
    factor = jnp.exp(got_peak - row_peak[None])
    totals_lat = jnp.sum(got_totals * factor, axis=0)
    weighted = jnp.sum(got_weighted * factor[..., None], axis=0)
    lat_out = (
        (weighted / totals_lat[..., None])
        .transpose(1, 0, 2)
        .reshape(tok_rows, head_count * VALUE_WIDTH)
    )
    lat_out = lat_out.astype(jnp.bfloat16)
    terms = jnp.dot(win_out, out_win, preferred_element_type=jnp.float32) + jnp.dot(
        lat_out, out_lat, preferred_element_type=jnp.float32
    )
    return sent_and_summed(terms.astype(jnp.bfloat16), "tp", 1).astype(jnp.bfloat16)


def solution(mesh):
    return jax.shard_map(
        per_device,
        mesh=mesh,
        in_specs=(
            P("sp", "tp"),
            P(),
            P(None, "tp"),
            P(None, "tp"),
            P(None, "tp"),
            P("tp"),
            P(None, "tp"),
            P(),
            P(),
            P(),
            P(None, "tp"),
            P(None, "tp"),
            P("tp", None),
            P("tp", None),
        ),
        out_specs=P("sp", "tp"),
        check_vma=False,
    )
```

profile of v0, /device:TPU:1, one launch (start us, length us, event | category | flops | bytes accessed | tf_op | source)
XLA Modules:
  0.0 243.2 jit_solution(10742603849364252246)
XLA Ops:
  0.0 1.1 copy.35
  1.1 1.0 broadcast_in_dim.16
  2.1 10.3 %all-to-all-start = ((bf16[8,256,256]{1,2,0:T(8,128)(2,1)}), bf16[8,256,256]{1,2,0:T(8,128)(2,1)S(1)}, u32[]{:S(2)}, u32[]{:S(2)}) async-start(bf16[8,256,256]{1,2,0:T(8,128)(2,1)} %broadcast_in_dim.16), calls=%async_computation | async-start | bytes 2097152 | tf_op jit(solution)/shard_map/all_to_all | solution.py:28
  13.1 0.9 fusion.41
  14.1 21.1 %all_gather.10 = bf16[256,1024]{1,0:T(8,128)(2,1)S(1)} all-gather(bf16[256,128]{1,0:T(8,128)(2,1)S(1)} %pad_maximum_fusion.3), channel_id=1, replica_groups=mesh['sp'=64,'tp'=8] {'tp'}, dimensions={1}, use_global_device_ids=true | all-gather | bytes 589824 | tf_op jit(solution)/shard_map/all_gather | solution.py:55
  35.2 1.0 fusion.38
  37.9 1.6 fusion.23
  40.1 13.6 %all_gather.11 = bf16[256,8,192]{0,2,1:T(8,128)(2,1)S(1)} all-gather(bf16[256,1,192]{0,2,1:T(8,128)(2,1)S(1)} %pad_maximum_fusion.2), channel_id=1, replica_groups=mesh['sp'=64,'tp'=8] {'tp'}, dimensions={1}, use_global_device_ids=true | all-gather | bytes 884736 | tf_op jit(solution)/shard_map/all_gather | solution.py:55
  53.7 0.8 split.26
  55.2 1.7 multiply_reduce_fusion.2
  57.1 77.7 %all_gather.9 = bf16[2048,192]{1,0:T(8,128)(2,1)S(1)} all-gather(bf16[32,192]{1,0:T(8,128)(2,1)S(1)} %pad_maximum_fusion.5), channel_id=1, replica_groups=mesh['sp'=64,'tp'=8] {'sp'}, dimensions={0}, use_global_device_ids=true | all-gather | bytes 798720 | tf_op jit(solution)/shard_map/all_gather | solution.py:55
  135.6 0.8 split.24
  137.1 1.0 fusion.28
  138.2 2.6 %collective-permute-start = (bf16[128,128]{0,1:T(8,128)(2,1)S(1)}, bf16[128,128]{0,1:T(8,128)(2,1)S(1)}, u32[]{:S(2)}, u32[]{:S(2)}) collective-permute-start(bf16[128,128]{0,1:T(8,128)(2,1)S(1)} %get-tuple-element.155), channel_id=1, source_target_pairs={{0,8},{8,16},{16,24},{24,32},{32,40},{40,48},{48,56},{56,64},{64,7... | collective-permute-start | bytes 98312 | tf_op jit(solution)/shard_map/ppermute | solution.py:43
  140.8 1.3 collective-permute-start.1
  142.1 1.3 copy.38
  143.4 1.2 copy.39
  144.7 36.6 %while.15 = (s32[]{:T(128)}, f32[8,256]{1,0:T(8,128)S(1)}, f32[8,256]{1,0:T(8,128)S(1)}, f32[8,256,128]{2,1,0:T(8,128)S(1)}, bf16[8,256,128]{2,1,0:T(8,128)(2,1)...) while((s32[]{:T(128)}, f32[8,256]{1,0:T(8,128)S(1)}, ...), condition=%wide.region_7.8_spmd.clone, body=%wide.region_4.7_spmd.clone.sunk | while | flops 474753024 | bytes 16285845 | solution.py:180
  144.7 1.1 fusion.129
  145.8 1.3 fusion.124
  148.3 0.9 convolution_add_fusion.3
  149.2 1.1 fusion.129
  150.4 1.3 fusion.124
  152.9 0.9 convolution_add_fusion.3
  153.8 1.1 fusion.129
  155.0 1.3 fusion.124
  157.5 0.9 convolution_add_fusion.3
  158.4 1.1 fusion.129
  159.5 1.3 fusion.124
  162.1 0.9 convolution_add_fusion.3
  163.0 1.1 fusion.129
  164.1 1.3 fusion.124
  166.6 0.9 convolution_add_fusion.3
  167.5 1.1 fusion.129
  168.7 1.3 fusion.124
  171.2 0.9 convolution_add_fusion.3
  172.1 1.1 fusion.129
  173.2 1.3 fusion.124
  175.8 0.9 convolution_add_fusion.3
  176.7 1.1 fusion.129
  177.8 1.3 fusion.124
  180.4 0.9 convolution_add_fusion.3
  181.5 1.0 pad_maximum_fusion
  182.5 29.2 %all-to-all-start.1 = ((bf16[1,8,256,130]{2,3,0,1:T(8,128)(2,1)}), bf16[1,8,256,130]{2,3,0,1:T(8,128)(2,1)S(1)}, u32[]{:S(2)}, u32[]{:S(2)}) async-start(bf16[1,8,256,130]{2,3,0,1:T(8,128)(2,1)} %pad_maximum_fusion), calls=%async_computation.1 | async-start | bytes 1114112 | tf_op jit(solution)/shard_map/all_to_all | solution.py:63
  212.8 1.8 fusion.79
  214.6 6.8 %all-to-all-done.1 = bf16[1,8,256,130]{2,3,0,1:T(8,128)(2,1)S(1)} async-done(((bf16[1,8,256,130]{2,3,0,1:T(8,128)(2,1)}), bf16[1,8,256,130]{2,3,0,1:T(8,128)(2,1)S(1)}, u32[]{:S(2)}, u32[]{:S(2)}) %all-to-all-start.1) | async-done | bytes 532512 | tf_op jit(solution)/shard_map/all_to_all | solution.py:63
  221.9 2.1 fusion.22
  224.1 18.3 %all_to_all.22 = bf16[8,256,256]{2,1,0:T(8,128)(2,1)S(1)} all-to-all(bf16[8,256,256]{2,1,0:T(8,128)(2,1)S(1)} %bitcast.158), channel_id=1, replica_groups=mesh['sp'=64,'tp'=8] {'tp'}, dimensions={0} | all-to-all | bytes 2097152 | tf_op jit(solution)/shard_map/all_to_all | solution.py:82
  (133 shorter events, 17.7 us)
Async XLA Ops:
  0.0 39.4 %copy-start = (bf16[2048,192]{0,1:T(8,128)(2,1)S(1)}, bf16[2048,192]{0,1:T(8,128)(2,1)}, u32[]{:S(2)}) copy-start(bf16[2048,192]{0,1:T(8,128)(2,1)} %param.22) | copy-start | bytes 2359300
  0.0 13.1 %copy-start.11 = (bf16[128,128]{1,0:T(8,128)(2,1)S(1)}, bf16[128,128]{1,0:T(8,128)(2,1)}, u32[]{:S(2)}) copy-start(bf16[128,128]{1,0:T(8,128)(2,1)} %param.27) | copy-start | bytes 98308
  0.0 13.1 %copy-start.12 = (bf16[128,128]{1,0:T(8,128)(2,1)S(1)}, bf16[128,128]{1,0:T(8,128)(2,1)}, u32[]{:S(2)}) copy-start(bf16[128,128]{1,0:T(8,128)(2,1)} %param.26) | copy-start | bytes 98308
  2.1 34.8 %all-to-all-start = ((bf16[8,256,256]{1,2,0:T(8,128)(2,1)}), bf16[8,256,256]{1,2,0:T(8,128)(2,1)S(1)}, u32[]{:S(2)}, u32[]{:S(2)}) async-start(bf16[8,256,256]{1,2,0:T(8,128)(2,1)} %broadcast_in_dim.16), calls=%async_computation | async-start | bytes 2097152 | tf_op jit(solution)/shard_map/all_to_all | solution.py:28
  12.4 25.5 %copy-start.13 = (f32[2048]{0:T(1024)S(1)}, f32[2048]{0:T(1024)}, u32[]{:S(2)}) copy-start(f32[2048]{0:T(1024)} %param.17) | copy-start | bytes 24580
  36.9 1.0 copy-start.1
  37.9 98.9 %copy-start.10 = (f32[256]{0:T(256)}, f32[256]{0:T(256)S(1)}, u32[]{:S(2)}) copy-start(f32[256]{0:T(256)S(1)} %add_rsqrt_fusion.1) | copy-start | bytes 3076
  39.5 15.1 %copy-start.6 = (bf16[2048,64]{0,1:T(8,128)(2,1)S(1)}, bf16[2048,64]{0,1:T(8,128)(2,1)}, u32[]{:S(2)}) copy-start(bf16[2048,64]{0,1:T(8,128)(2,1)} %param.24) | copy-start | bytes 786436
  53.7 3.3 %copy-start.15 = (f32[128]{0:T(128)S(1)}, f32[128]{0:T(128)}, u32[]{:S(2)}) copy-start(f32[128]{0:T(128)} %param.25) | copy-start | bytes 1540
  55.2 81.2 %copy-start.7 = (bf16[2048,64]{0,1:T(8,128)(2,1)S(1)}, bf16[2048,64]{0,1:T(8,128)(2,1)}, u32[]{:S(2)}) copy-start(bf16[2048,64]{0,1:T(8,128)(2,1)} %param.20) | copy-start | bytes 786436
  57.1 79.7 %copy-start.8 = (bf16[2048,64]{0,1:T(8,128)(2,1)S(1)}, bf16[2048,64]{0,1:T(8,128)(2,1)}, u32[]{:S(2)}) copy-start(bf16[2048,64]{0,1:T(8,128)(2,1)} %param.19) | copy-start | bytes 786436
  135.6 1.5 copy-start.3
  138.2 73.5 %collective-permute-start = (bf16[128,128]{0,1:T(8,128)(2,1)S(1)}, bf16[128,128]{0,1:T(8,128)(2,1)S(1)}, u32[]{:S(2)}, u32[]{:S(2)}) collective-permute-start(bf16[128,128]{0,1:T(8,128)(2,1)S(1)} %get-tuple-element.155), channel_id=1, source_target_pairs={{0,8},{8,16},{16,24},{24,32},{32,40},{40,48},{48,56},{56,64},{64,7... | collective-permute-start | bytes 98312 | tf_op jit(solution)/shard_map/ppermute | solution.py:43
  140.8 70.9 %collective-permute-start.1 = (bf16[128,128]{0,1:T(8,128)(2,1)S(1)}, bf16[128,128]{0,1:T(8,128)(2,1)S(1)}, u32[]{:S(2)}, u32[]{:S(2)}) collective-permute-start(bf16[128,128]{0,1:T(8,128)(2,1)S(1)} %get-tuple-element.156), channel_id=1, source_target_pairs={{8,0},{16,8},{24,16},{32,24},{40,32},{48,40},{56,48},{64,56},{72,6... | collective-permute-start | bytes 98312 | tf_op jit(solution)/shard_map/ppermute | solution.py:45
  181.2 30.5 %copy-start.2 = (f32[256,512]{0,1:T(8,128)S(1)}, f32[256,512]{0,1:T(8,128)}, u32[]{:S(2)}) copy-start(f32[256,512]{0,1:T(8,128)} %fusion.38) | copy-start | bytes 1572868
  181.3 30.5 %copy-start.9 = (pred[256,512]{0,1:T(8,128)(4,1)S(1)}, pred[256,512]{0,1:T(8,128)(4,1)}, u32[]{:S(2)}) copy-start(pred[256,512]{0,1:T(8,128)(4,1)} %fusion.41) | copy-start | bytes 393220
  181.3 30.5 %copy-start.16 = (f32[2]{0:T(128)S(1)}, f32[2]{0:T(128)}, u32[]{:S(2)}) copy-start(f32[2]{0:T(128)} %multiply_exponential_fusion) | copy-start | bytes 28
  181.5 30.6 %copy-start.14 = (f32[2]{0:T(128)S(1)}, f32[2]{0:T(128)}, u32[]{:S(2)}) copy-start(f32[2]{0:T(128)} %param.21) | copy-start | bytes 28
  182.5 38.9 %all-to-all-start.1 = ((bf16[1,8,256,130]{2,3,0,1:T(8,128)(2,1)}), bf16[1,8,256,130]{2,3,0,1:T(8,128)(2,1)S(1)}, u32[]{:S(2)}, u32[]{:S(2)}) async-start(bf16[1,8,256,130]{2,3,0,1:T(8,128)(2,1)} %pad_maximum_fusion), calls=%async_computation.1 | async-start | bytes 1114112 | tf_op jit(solution)/shard_map/all_to_all | solution.py:63
  211.7 1.1 copy-start.4
  212.8 9.1 %copy-start.5 = (bf16[128,2048]{1,0:T(8,128)(2,1)S(1)}, bf16[128,2048]{1,0:T(8,128)(2,1)}, u32[]{:S(2)}) copy-start(bf16[128,2048]{1,0:T(8,128)(2,1)} %param.29) | copy-start | bytes 1572868
where the time goes:
time: 247 us; the launch traced here: 243 us
  blocking collectives  131 us (53%)
  starting transfers between devices  43.4 us (18%)
  matrix products  41.9 us (17%)
  other arithmetic  10 us (4%)
  local copies, waits for them, and re-layouts  9.22 us (4%)
  waiting for transfers between devices  6.84 us (3%)
    all_gather x3, blocking collectives, in_one_piece(): whole = lax.all_gather(both, axis, axis=dim, tiled=True)  112 us
    all_to_all x1, starting transfers between devices, sent_together(): lax.all_to_all(both, axis, split_axis=split_dim, concat_axis=concat_dim,...  29.2 us
    all_to_all x1, blocking collectives, sent_and_summed(): lax.all_to_all(tiles, axis, split_axis=0, concat_axis=0, tiled=True)  18.3 us
    all_to_all x1, starting transfers between devices, from_everyone(): return lax.all_to_all(copies, axis, split_axis=0, concat_axis=0, tiled=True)  10.3 us
    dot_general x8, matrix products, expand_all(): jnp.dot(key_block[0], key_up_all, preferred_element_type=jnp.float32)  10.2 us
    dot_general x8, matrix products, expand_all(): jnp.dot(key_block[0], value_up_all, preferred_element_type=jnp.float32)  9.02 us
    dot_general x8, matrix products, latent_step(): jnp.einsum('hqk,khd->hqd', weights.astype(jnp.bfloat16), values_plain.res...  6.95 us
    all_to_all x1, waiting for transfers between devices, sent_together(): lax.all_to_all(both, axis, split_axis=split_dim, concat_axis=concat_dim,...  6.83 us
  transfers between devices with their start and end apart: 4, of which 1 were waited for; matrix products, arithmetic and copies ran while one was open for 19% of the time, Pallas kernels for 0%

commit v1 on v0

v1 whole, which is shorter than its diff:
```python
import functools

import jax
import jax.numpy as jnp
import numpy as np
from jax import lax
from jax.experimental import pallas as pl
from jax.experimental.pallas import tpu as pltpu
from jax.sharding import PartitionSpec as P

HEADS_A = 16
DH = 64
WINDOW = 128
PLAIN = 128
D_ROPE = 64
EPSILON = 1e-06
ROPE_BASE = 10000.0
NY = 4
REACH = 4
LOG2E = 1.4426950408889634
MESH = pl.DeviceIdType.MESH
BF16 = jnp.bfloat16
F32 = jnp.float32

NT = (((1,), (1,)), ((), ()))
TN = (((0,), (0,)), ((), ()))


def mm(a, b, dims=(((1,), (0,)), ((), ()))):
    return lax.dot_general(a, b, dims, preferred_element_type=F32)


def z_plan(nz):
    if nz == 4 * REACH:
        near = [REACH, -REACH]
        for k in range(1, REACH):
            near += [k, -k]
        return near, list(range(1, REACH + 1))[::-1], [-k for k in range(1, REACH)][::-1]
    half = nz // 2
    near = []
    for k in range(1, half + 1):
        near.append(k)
        if k != nz - k:
            near.append(-k)
    return near, [], []


def rotate(u, cos, sin):
    half = u.shape[1] // 2
    a, b = u[:, :half], u[:, half:]
    return jnp.concatenate([a * cos - b * sin, a * sin + b * cos], axis=1)


def kernel(
    cfg,
    act, gain, wq, wk, wv, sink, wlq, wkvd, wrope, lgain, kup, vup, ow, ol, ta, tb,
    out,
    actv, gv, lgv, tav, tbv, sinkv, wqv, wkv, wvv, wlqv, kdv, krv, kupv, vupv, wall,
    kps, kpr, xb, accq, acck, accv, accl, sqv,
    kbuf, qt, kvb, catt, cat, mst, lst, acc, pos, por, pls, plr, rss, rsr,
    lsem, wssem, wrsem, kpssem, kprsem, xssem, xrsem, kzs, kzr, kys, kyr, kds, kdr,
    qss, qrs, hss, hrs, pss, prs, lss, lrs, rs_s, rs_r,
):
    nz, ny, nx, tok, ft, model = cfg
    tp = 2 * nx
    ht = tok // 2
    sl = tok // tp
    s = lax.axis_index("sp")
    t = lax.axis_index("tp")
    sp = nz * ny
    z, y = s // ny, lax.rem(s, ny)
    x, c = t // 2, lax.rem(t, 2)
    other = 1 - c
    mate = t + 1 - 2 * c

    near, fwd_up, fwd_down = z_plan(nz)

    def at_z(dz):
        return lax.rem(z + dz + nz, nz)

    def at_y(dy):
        return lax.rem(y + dy + ny, ny)

    def rc(src, dst, ss, rs, sp_id, tp_id):
        return pltpu.make_async_remote_copy(
            src_ref=src, dst_ref=dst, send_sem=ss, recv_sem=rs,
            device_id=(sp_id, tp_id), device_id_type=MESH,
        )

    def done(ref, sem):
        pltpu.make_async_copy(ref, ref, sem).wait()

    rows = pl.ds(pl.multiple_of(t * ft, ft), ft)
    loads = [
        (act, actv), (gain, gv), (wkvd.at[rows], kdv), (wrope.at[rows], krv),
        (lgain, lgv), (ta, tav), (tb, tbv),
        (wq, wqv.at[c]), (wk, wkv.at[c]), (wv, wvv.at[c]), (wlq, wlqv.at[c]),
        (kup, kupv.at[c]), (vup, vupv.at[c]), (ow, wall.at[c]), (ol, wall.at[2 + c]),
    ]
    local = [pltpu.make_async_copy(a, b, lsem.at[i]) for i, (a, b) in enumerate(loads)]
    for copy in local:
        copy.start()

    own_sink = jnp.concatenate(
        [jnp.full((8, 128), sink[0], F32), jnp.full((8, 128), sink[1], F32)], axis=1
    )
    sinkv[c] = own_sink

    barrier = pltpu.get_barrier_semaphore()
    n_sig = 0

    def greet(sp_id, tp_id):
        pl.semaphore_signal(barrier, inc=1, device_id=(sp_id, tp_id), device_id_type=MESH)

    for d in range(1, tp):
        greet(s, lax.rem(t + d, tp))
        n_sig += 1
    for dz in near:
        greet(at_z(dz) * ny + y, t)
        n_sig += 1
    for dy in range(1, ny):
        greet(z * ny + at_y(dy), t)
        n_sig += 1
    side = lax.rem(s + 2 * c - 1 + sp, sp)
    greet(side, mate)
    n_sig += 1
    for i in range(4):
        local[i].wait()
    xn = actv[...].astype(F32)
    sq0 = jnp.sum(xn * xn, axis=1, keepdims=True)
    xn = (xn * gv[pl.ds(t, 1), :]).astype(BF16)
    kps[...] = jnp.concatenate(
        [mm(xn, kdv[...]), mm(xn, krv[...]), jnp.broadcast_to(sq0, (tok, D_ROPE))], axis=1
    ).reshape(tp, sl, 256)
    kpr[pl.ds(t, 1)] = kps[pl.ds(t, 1)]
    pl.semaphore_wait(barrier, n_sig)

    def order(d):
        hop = d // 2 + 1
        if nx == 4:
            hop = jnp.where(hop == 3, 3, 3 - hop)
        return jnp.where(d < tp - 2, lax.rem((x + hop) * 2 + lax.rem(c + d, 2), tp), mate)

    def send_kp(d, _):
        j = order(d)
        rc(kps.at[j], kpr.at[t], kpssem.at[d], kprsem.at[t], s, j).start()
        return 0

    lax.fori_loop(0, tp - 1, send_kp, 0)

    def send_x(d, _):
        j = order(d)
        half = pl.ds(pl.multiple_of(lax.rem(j, 2) * ht, ht), ht)
        rc(actv.at[half], xb.at[t], xssem.at[d], xrsem.at[t], s, j).start()
        return 0

    lax.fori_loop(0, tp - 1, send_x, 0)
    wsends = [
        (wq, wqv.at[c]), (wk, wkv.at[c]), (wv, wvv.at[c]), (wlq, wlqv.at[c]),
        (kup, kupv.at[c]), (vup, vupv.at[c]), (ow, wall.at[c]), (ol, wall.at[2 + c]),
        (sinkv.at[c], sinkv.at[c]),
    ]
    wdone = [
        wqv.at[other], wkv.at[other], wvv.at[other], wlqv.at[other], kupv.at[other],
        vupv.at[other], wall.at[other], wall.at[2 + other], sinkv.at[other],
    ]
    wcopies = [
        rc(a, b, wssem.at[i], wrsem.at[i], s, mate) for i, (a, b) in enumerate(wsends)
    ]
    for copy in wcopies:
        copy.start()

    for i in range(4, 7):
        local[i].wait()
    cos_a, sin_a = tav[pl.ds(s, 1), 0:32], tav[pl.ds(s, 1), 32:64]

    def angles(start, count):
        at = pl.ds(pl.multiple_of(start, count), count)
        cos_b, sin_b = tbv[at, 0:32], tbv[at, 32:64]
        return cos_a * cos_b - sin_a * sin_b, sin_a * cos_b + cos_a * sin_b

    def wait_kp(d, _):
        j = order(d)
        done(kpr.at[j], kprsem.at[j])
        return 0

    lax.fori_loop(0, tp - 1, wait_kp, 0)
    tot = kpr[0]
    for j in range(1, tp):
        tot = tot + kpr[j]
    comp, rope, sqs = tot[:, :128], tot[:, 128:192], tot[:, 192:193]
    lat = comp * lax.rsqrt(jnp.mean(comp * comp, axis=1, keepdims=True) + EPSILON) * lgv[...]
    kcos, ksin = angles(t * sl, sl)
    kro = rotate(rope * lax.rsqrt(sqs / model + EPSILON), kcos, ksin)
    chunk = jnp.concatenate(
        [lat, jnp.concatenate([kro[: sl // 2], kro[sl // 2 :]], axis=1)], axis=0
    ).astype(BF16)
    kbuf[z, c, y] = chunk

    def z_send(dz, zs, sem):
        rc(kbuf.at[zs, c, y], kbuf.at[zs, c, y], kzs.at[sem], kzr.at[zs],
           at_z(dz) * ny + y, t).start()

    for i, dz in enumerate(near):
        z_send(dz, z, i)

    def y_send(zs):
        for dy in range(1, ny):
            rc(kbuf.at[zs, c, y], kbuf.at[zs, c, y], kys.at[zs, dy - 1], kyr.at[zs],
               z * ny + at_y(dy), t).start()

    def step_a(dz):
        zs = at_z(dz)
        if not (isinstance(dz, int) and dz == 0):
            done(kbuf.at[zs, c, y], kzr.at[zs])
        y_send(zs)

    def step_b(dz):
        zs = at_z(dz)
        if ny > 1:
            done(kbuf.at[zs, c, pl.ds(0, ny - 1)], kyr.at[zs])
        rc(kbuf.at[zs, c], kbuf.at[zs, c], kds.at[zs], kdr.at[zs], s, mate).start()

    step_a(0)

    for i in range(7, 11):
        local[i].wait()
    for i in range(4):
        done(wdone[i], wrsem.at[i])

    def project(xk, k, first):
        xf = xk.astype(F32)
        sq = jnp.sum(xf * xf, axis=1, keepdims=True)
        xk = (xf * gv[pl.ds(k, 1), :]).astype(BF16)
        kr = pl.ds(pl.multiple_of(k * ft, ft), ft)
        for c2 in range(2):
            for a, w in ((accq, wqv), (acck, wkv), (accv, wvv), (accl, wlqv)):
                term = mm(xk, w[c2, kr, :])
                a[c2] = term if first else a[c2] + term
        sqv[...] = sq if first else sqv[...] + sq

    own_half = pl.ds(pl.multiple_of(c * ht, ht), ht)
    project(actv[own_half, :], t, True)

    def project_next(d, _):
        k = order(tp - 2 - d)
        done(xb.at[k], xrsem.at[k])
        project(xb[k], k, False)
        return 0

    lax.fori_loop(0, tp - 1, project_next, 0)

    scale = lax.rsqrt(sqv[...] / model + EPSILON)
    local[11].wait()
    done(wdone[4], wrsem.at[4])
    qcos, qsin = angles(c * ht, ht)
    factor = (PLAIN + D_ROPE) ** (-0.5) * LOG2E
    for c2 in range(2):
        ql = accl[c2] * scale
        plain = ql[:, :PLAIN].astype(BF16)
        qt[x, 0:128, c2 * ht : (c2 + 1) * ht] = (mm(kupv[c2], plain, NT) * factor).astype(BF16)
        turned = rotate(ql[:, PLAIN:], qcos, qsin) * factor
        qt[x, 128:192, c2 * ht : (c2 + 1) * ht] = jnp.transpose(turned).astype(BF16)
    for dx in range(1, nx):
        xo = lax.rem(x + dx, nx)
        rc(qt.at[x], qt.at[x], qss.at[dx - 1], qrs.at[x], s, xo * 2 + c).start()

    for c2 in range(2):
        kvb[1, c2, :, 0:64] = (acck[c2] * scale).astype(BF16)
        kvb[1, c2, :, 64:128] = (accv[c2] * scale).astype(BF16)
    to_mate = rc(kvb.at[1], kvb.at[2 * c], hss.at[0], hrs.at[2 * c], s, mate)
    to_mate.start()
    to_side = rc(kvb.at[1], kvb.at[2 * other], hss.at[1], hrs.at[2 * other], side, mate)
    to_side.start()

    if fwd_up:
        zs = at_z(-REACH)
        done(kbuf.at[zs, c, y], kzr.at[zs])
        for i, dz in enumerate(fwd_up):
            z_send(dz, zs, len(near) + i)
        y_send(zs)
        zs = at_z(REACH)
        done(kbuf.at[zs, c, y], kzr.at[zs])
        for i, dz in enumerate(fwd_down):
            z_send(dz, zs, len(near) + len(fwd_up) + i)
        y_send(zs)
        first = [dz for dz in near if abs(dz) != REACH]
        late = [-(REACH + k) for k in fwd_up[::-1]] + [REACH - k for k in fwd_down[::-1]]
        late.sort(key=abs)
        seen = [0] + first + [-REACH, REACH]
    else:
        first, late, seen = [-dz for dz in near], [], [0] + [-dz for dz in near]
    for dz in first:
        step_a(dz)
    for dz in seen:
        step_b(dz)

    for i in (0, 2):
        done(kvb.at[i], hrs.at[i])
    done(wdone[8], wrsem.at[8])
    kpos = lax.broadcasted_iota(jnp.int32, (3 * ht, ht), 0)
    qpos = lax.broadcasted_iota(jnp.int32, (3 * ht, ht), 1)
    apart = jnp.abs(qpos + ht - kpos)
    place = kpos + (s * 2 + c - 1) * ht
    inside = (apart <= WINDOW) & (place >= 0) & (place < sp * tok)
    apart = apart.astype(F32)
    for c2 in range(2):
        kw = kvb[:, c2, :, 0:64].reshape(3 * ht, DH)
        vw = kvb[:, c2, :, 64:128].reshape(3 * ht, DH)
        qw = (accq[c2] * scale).astype(BF16)
        for g in range(2):
            head = (x * 2 + c2) * 2 + g
            slope = jnp.exp2(
                jnp.full((1, ht), -8.0 / (2 * tp), F32) * (head + 1).astype(F32)
            )
            sc = mm(kw, qw[:, g * DH : (g + 1) * DH], NT) * DH ** (-0.5) - slope * apart
            sc = jnp.where(inside, sc, -jnp.inf)
            snk = sinkv[c2, 0:1, g * 128 : g * 128 + 128]
            peak = jnp.maximum(jnp.max(sc, axis=0, keepdims=True), snk)
            w = jnp.exp(sc - peak)
            den = jnp.sum(w, axis=0, keepdims=True) + jnp.exp(snk - peak)
            o = mm(vw, w.astype(BF16), TN) / den
            catt[(c2 * 2 + g) * DH : (c2 * 2 + g + 1) * DH, :] = o.astype(BF16)

    for dz in late:
        step_a(dz)
    for dz in late:
        step_b(dz)

    for dx in range(1, nx):
        xo = lax.rem(x + dx, nx)
        done(qt.at[xo], qrs.at[xo])
    mst[...] = jnp.full(mst.shape, -jnp.inf, F32)
    lst[...] = jnp.zeros(lst.shape, F32)
    acc[...] = jnp.zeros(acc.shape, F32)
    nkeys = 2 * ny * sl

    def batch(j, _):
        near_j = (j + 1) // 2
        dz = jnp.where(lax.rem(j, 2) == 0, near_j, -near_j)
        zs = lax.rem(z + dz + nz, nz)
        done(kbuf.at[zs, other], kdr.at[zs])
        both = kbuf[zs].reshape(2 * ny, sl + sl // 2, 128)
        latk = both[:, :sl, :].reshape(nkeys, 128)
        rp = both[:, sl:, :]
        rk = jnp.concatenate([rp[:, :, 0:64], rp[:, :, 64:128]], axis=1).reshape(nkeys, 64)
        keys = jnp.concatenate([latk, rk], axis=1)
        latt = jnp.transpose(latk)
        for xp in range(nx):
            sc = mm(keys, qt[xp])
            m_old = mst[xp]
            m_new = jnp.maximum(m_old, jnp.max(sc, axis=0, keepdims=True))
            alpha = jnp.exp2(m_old - m_new)
            p = jnp.exp2(sc - m_new)
            mst[xp] = m_new
            lst[xp] = lst[xp] * alpha + jnp.sum(p, axis=0, keepdims=True)
            acc[xp] = acc[xp] * alpha + mm(latt, p.astype(BF16))
        return 0

    lax.fori_loop(0, nz, batch, 0)

    for xp in range(nx):
        l = lst[xp]
        pos[xp] = (acc[xp] / l).astype(BF16)
        pls[xp] = jnp.broadcast_to(mst[xp] + jnp.log(l) * LOG2E, (8, 2 * ht))
    for dx in range(1, nx):
        xo = lax.rem(x + dx, nx)
        rc(pls.at[xo], plr.at[x], lss.at[dx - 1], lrs.at[x], s, xo * 2 + c).start()
        rc(pos.at[xo], por.at[x], pss.at[dx - 1], prs.at[x], s, xo * 2 + c).start()
    por[pl.ds(x, 1)] = pos[pl.ds(x, 1)]
    plr[pl.ds(x, 1)] = pls[pl.ds(x, 1)]
    for i in range(12, 15):
        local[i].wait()
    for i in range(5, 8):
        done(wdone[i], wrsem.at[i])
    for dx in range(1, nx):
        xo = lax.rem(x + dx, nx)
        done(plr.at[xo], lrs.at[xo])
        done(por.at[xo], prs.at[xo])
    lse = [plr[xp, 0:1, :] for xp in range(nx)]
    top = functools.reduce(jnp.maximum, lse)
    wts = [jnp.exp2(v - top) for v in lse]
    total = functools.reduce(lambda a, b: a + b, wts)
    mixed = por[0].astype(F32) * wts[0]
    for xp in range(1, nx):
        mixed = mixed + por[xp].astype(F32) * wts[xp]
    mixed = (mixed / total).astype(BF16)
    for h in range(2):
        catt[256 + h * 128 : 256 + (h + 1) * 128, :] = mm(
            vupv[h], mixed[:, h * ht : (h + 1) * ht], TN
        ).astype(BF16)
    cat[...] = jnp.transpose(catt[...])

    def out_block(d, _):
        j = order(d)
        cols = pl.ds(pl.multiple_of(j * ft, ft), ft)
        o = mm(cat[:, 0:128], wall[0, :, cols])
        for i in range(1, 4):
            o = o + mm(cat[:, i * 128 : (i + 1) * 128], wall[i, :, cols])
        rss[j] = o.astype(BF16)
        return j

    def send_block(d, _):
        j = out_block(d, _)
        rc(rss.at[j], rsr.at[x, c], rs_s.at[d], rs_r.at[x, c], s, j).start()
        return 0

    lax.fori_loop(0, tp - 1, send_block, 0)
    cols = pl.ds(pl.multiple_of(t * ft, ft), ft)
    o = mm(cat[:, 0:128], wall[0, :, cols])
    for i in range(1, 4):
        o = o + mm(cat[:, i * 128 : (i + 1) * 128], wall[i, :, cols])
    rsr[x, c] = o.astype(BF16)

    def wait_block(d, _):
        j = order(tp - 2 - d)
        jx, jc = j // 2, lax.rem(j, 2)
        done(rsr.at[jx, jc], rs_r.at[jx, jc])
        return 0

    lax.fori_loop(0, tp - 1, wait_block, 0)
    for c2 in range(2):
        total = rsr[0, c2].astype(F32)
        for xp in range(1, nx):
            total = total + rsr[xp, c2].astype(F32)
        out[c2 * ht : (c2 + 1) * ht, :] = total.astype(BF16)

    def sent(d, _):
        done(kps.at[0], kpssem.at[d])
        done(xb.at[0], xssem.at[d])
        done(rss.at[0], rs_s.at[d])
        return 0

    lax.fori_loop(0, tp - 1, sent, 0)
    for copy in wcopies:
        copy.wait_send()
    for i in range(len(near) + len(fwd_up) + len(fwd_down)):
        done(kbuf.at[0, 0, 0], kzs.at[i])

    def sent_keys(zs, _):
        for dy in range(ny - 1):
            done(kbuf.at[0, 0, 0], kys.at[zs, dy])
        done(kbuf.at[0, 0], kds.at[zs])
        return 0

    lax.fori_loop(0, nz, sent_keys, 0)
    for i in range(nx - 1):
        done(qt.at[0], qss.at[i])
        done(pls.at[0], lss.at[i])
        done(pos.at[0], pss.at[i])
    to_mate.wait_send()
    to_side.wait_send()


def tables(sp, tok):
    freq = 1.0 / ROPE_BASE ** (np.arange(0, D_ROPE, 2, dtype=np.float64) / D_ROPE)

    def table(places):
        angle = places[:, None] * freq[None, :]
        flat = np.concatenate([np.cos(angle), np.sin(angle)], axis=1)
        return np.pad(flat, ((0, 0), (0, 64))).astype(np.float32)

    return table(np.arange(sp) * float(tok)), table(np.arange(tok) * 1.0)


def per_device(nz, *args):
    (act, gain, wq, wk, wv, sink, wlq, wkvd, wrope, lgain, kup, vup, ow, ol) = args
    tp, sp = lax.axis_size("tp"), lax.axis_size("sp")
    nx = tp // 2
    ny = sp // nz
    tok, ft = act.shape
    model = tp * ft
    ht, sl = tok // 2, tok // tp
    ta, tb = tables(sp, tok)
    cfg = (nz, ny, nx, tok, ft, model)
    near, up, down = z_plan(nz)
    n_z = len(near) + len(up) + len(down)
    dma = pltpu.SemaphoreType.DMA
    v = pltpu.VMEM
    scratch = [
        v((tok, ft), BF16), v((tp, ft), F32), v((1, 128), F32), v((sp, 128), F32),
        v((tok, 128), F32), v((2, 8, 256), F32), v((2, model, 128), BF16),
        v((2, model, 64), BF16), v((2, model, 64), BF16), v((2, model, 192), BF16),
        v((ft, 128), BF16), v((ft, 64), BF16), v((2, 128, 128), BF16), v((2, 128, 128), BF16),
        v((4, 128, model), BF16),
        v((tp, sl, 256), F32), v((tp, sl, 256), F32), v((tp, ht, ft), BF16),
        v((2, ht, 128), F32), v((2, ht, 64), F32), v((2, ht, 64), F32), v((2, ht, 192), F32),
        v((ht, 1), F32),
        v((nz, 2, ny, sl + sl // 2, 128), BF16), v((nx, 192, 2 * ht), BF16),
        v((3, 2, ht, 128), BF16), v((512, ht), BF16), v((ht, 512), BF16),
        v((nx, 1, 2 * ht), F32), v((nx, 1, 2 * ht), F32), v((nx, 128, 2 * ht), F32),
        v((nx, 128, 2 * ht), BF16), v((nx, 128, 2 * ht), BF16),
        v((nx, 8, 2 * ht), F32), v((nx, 8, 2 * ht), F32),
        v((tp, ht, ft), BF16), v((nx, 2, ht, ft), BF16),
        dma((15,)), dma((9,)), dma((9,)), dma((tp,)), dma((tp,)), dma((tp,)), dma((tp,)),
        dma((n_z,)), dma((nz,)), dma((nz, max(ny - 1, 1))), dma((nz,)), dma((nz,)), dma((nz,)),
        dma((nx,)), dma((nx,)), dma((2,)), dma((3,)), dma((nx,)), dma((nx,)), dma((nx,)), dma((nx,)),
        dma((tp,)), dma((nx, 2)),
    ]
    hbm = pl.BlockSpec(memory_space=pl.ANY)
    specs = [hbm] * 16
    specs[5] = pl.BlockSpec(memory_space=pltpu.SMEM)
    return pl.pallas_call(
        functools.partial(kernel, cfg),
        out_shape=jax.ShapeDtypeStruct((tok, ft), BF16),
        in_specs=specs,
        out_specs=pl.BlockSpec(memory_space=pltpu.VMEM),
        scratch_shapes=scratch,
        compiler_params=pltpu.CompilerParams(
            collective_id=0, has_side_effects=True, vmem_limit_bytes=48 * 1024 * 1024
        ),
    )(
        act, gain.reshape(tp, ft), wq, wk, wv, sink, wlq, wkvd, wrope,
        lgain.reshape(1, 128), kup, vup, ow, ol, jnp.asarray(ta), jnp.asarray(tb),
    )


def solution(mesh):
    return jax.shard_map(
        functools.partial(per_device, mesh.shape["sp"] // NY),
        mesh=mesh,
        in_specs=(
            P("sp", "tp"), P(), P(None, "tp"), P(None, "tp"), P(None, "tp"), P("tp"),
            P(None, "tp"), P(), P(), P(), P(None, "tp"), P(None, "tp"), P("tp", None),
            P("tp", None),
        ),
        out_specs=P("sp", "tp"),
        check_vma=False,
    )
```

time: 247 us -> 87.2 us (0.35); the launches traced: 243 us -> 86.4 us
  blocking collectives: 131 us -> 0 us
  Pallas kernels: 0 us -> 77.7 us
  starting transfers between devices: 43.4 us -> 0 us
  matrix products: 41.9 us -> 0 us
  other arithmetic: 10 us -> 0 us
  waiting for transfers between devices: 6.84 us -> 0 us
    all_gather x3 -> x0, blocking collectives: 112 us -> none  [in_one_piece(): whole = lax.all_gather(both, axis, axis=dim, tiled=True)]
    pallas_call x0 -> x1, Pallas kernels: none -> 77.7 us  [per_device(): pl.pallas_call(functools.partial(kernel, cfg), out_shape=jax.ShapeDtypeSt...]
    dot_general x50 -> x0, matrix products: 41.9 us -> none  [the longest x8 10.2 us: expand_all(): jnp.dot(key_block[0], key_up_all, preferred_element_type=jnp.float32)]
    all_to_all x2 -> x0, starting transfers between devices: 39.5 us -> none  [the longest x1 29.2 us: sent_together(): lax.all_to_all(both, axis, split_axis=split_dim, concat_axis=concat_dim,...]
    all_to_all x1 -> x0, blocking collectives: 18.3 us -> none  [sent_and_summed(): lax.all_to_all(tiles, axis, split_axis=0, concat_axis=0, tiled=True)]
    all_to_all x2 -> x0, waiting for transfers between devices: 6.84 us -> none  [the longest x1 6.83 us: sent_together(): lax.all_to_all(both, axis, split_axis=split_dim, concat_axis=concat_dim,...]
    reduce_sum x13 -> x0, other arithmetic: 3.99 us -> none  [the longest x8 2.35 us: latent_step(): totals = totals * factor + jnp.sum(weights, axis=2)]
    ppermute x2 -> x0, starting transfers between devices: 3.93 us -> none  [the longest x1 2.64 us: padded_2(): lax.ppermute(tail, axis, [(i, (i + 1) % count) for i in range(ends)])]
  transfers between devices with their start and end apart: 4 -> 0, of which waited for: 1 -> 0; matrix products, arithmetic and copies ran while one was open for 19% -> 0% of each run, Pallas kernels for 0% -> 0%
where the time goes in v1:
time: 87.2 us; the launch traced here: 86.4 us
  Pallas kernels  77.7 us (89%)
  local copies, waits for them, and re-layouts  8.5 us (10%)
    pallas_call x1, Pallas kernels, per_device(): pl.pallas_call(functools.partial(kernel, cfg), out_shape=jax.ShapeDtypeSt...  77.7 us
    unnamed x31, local copies, waits for them, and re-layouts  7.8 us

profile of v1, /device:TPU:1, one launch (start us, length us, event | category | flops | bytes accessed | tf_op | source)
XLA Modules:
  0.0 86.4 jit_solution(16619840746124457051)
XLA Ops:
  0.0 0.7 reshape.6.gain
  0.7 0.0 copy-start.11
  0.7 1.3 %copy.17.wk = bf16[2048,64]{1,0:T(8,128)(2,1)S(1)} copy(bf16[2048,64]{0,1:T(8,128)(2,1)} %param.19) | data formatting | bytes 524288 | tf_op args[3]
  2.0 0.0 copy-done.11
  2.0 0.0 copy-start.12
  2.0 0.3 copy.18.wv
  2.3 0.7 copy-done.12
  2.9 0.3 copy.20.wrope
  3.2 0.0 copy-start
  3.2 0.0 copy-start.4
  3.2 0.0 copy-start.5
  3.3 0.0 copy-start.6
  3.3 0.0 copy-start.7
  3.3 0.0 copy-start.8
  3.3 0.0 copy-start.9
  3.3 0.0 copy-start.10
  3.3 1.5 %copy.19.wlq = bf16[2048,192]{1,0:T(8,128)(2,1)S(1)} copy(bf16[2048,192]{0,1:T(8,128)(2,1)} %param.22) | data formatting | bytes 1572864 | tf_op args[6]
  4.8 0.0 copy-done
  4.8 0.0 copy-done.4
  4.8 0.0 copy-done.5
  4.8 0.0 copy-done.6
  4.9 0.0 copy-done.7
  4.9 0.0 copy-done.8
  4.9 0.0 copy-done.9
  4.9 0.0 copy-done.10
  4.9 0.0 copy-start.1
  4.9 1.0 %copy-done.1 = bf16[2048,128]{1,0:T(8,128)(2,1)S(1)} copy-done((bf16[2048,128]{1,0:T(8,128)(2,1)S(1)}, bf16[2048,128]{1,0:T(8,128)(2,1)}, u32[]{:S(2)}) %copy-start.1) | copy-done | bytes 524312
  5.9 0.0 copy-start.2
  5.9 1.0 %copy-done.2 = bf16[128,2048]{1,0:T(8,128)(2,1)S(1)} copy-done((bf16[128,2048]{1,0:T(8,128)(2,1)S(1)}, bf16[128,2048]{1,0:T(8,128)(2,1)}, u32[]{:S(2)}) %copy-start.2) | copy-done | bytes 524312
  7.0 0.0 copy-start.3
  7.0 1.0 %copy-done.3 = bf16[128,2048]{1,0:T(8,128)(2,1)S(1)} copy-done((bf16[128,2048]{1,0:T(8,128)(2,1)S(1)}, bf16[128,2048]{1,0:T(8,128)(2,1)}, u32[]{:S(2)}) %copy-start.3) | copy-done | bytes 524312
  8.0 77.7 %shard_map.154 = bf16[256,256]{1,0:T(8,128)(2,1)S(1)} custom-call(bf16[256,256]{1,0:T(8,128)(2,1)S(1)} %copy-done.4, f32[8,256]{1,0:T(8,128)S(1)} %reshape.6.gain, bf16[2048,128]{1,0:T(8,128)(2,1)S(1)} %copy-done, bf16[2048,64]{1,0:T(8,128)(2,1)S(1)} %copy.17.wk, bf16[2048,64]{1,0:T(8,128)(2,1)S(1)} %copy.18.wv, f32[2]{0:T(128)S(1)} %copy-done.9, ...), custom_call_target="tpu_custom_call" | custom-call | tf_op jit(solution)/shard_map/pallas_call | solution.py:503
  85.7 0.7 copy.22
Async XLA Ops:
  0.7 1.3 %copy-start.11 = (bf16[2048,64]{0,1:T(8,128)(2,1)S(1)}, bf16[2048,64]{0,1:T(8,128)(2,1)}, u32[]{:S(2)}) copy-start(bf16[2048,64]{0,1:T(8,128)(2,1)} %param.20) | copy-start | bytes 786436
  2.0 1.0 %copy-start.12 = (bf16[2048,64]{0,1:T(8,128)(2,1)S(1)}, bf16[2048,64]{0,1:T(8,128)(2,1)}, u32[]{:S(2)}) copy-start(bf16[2048,64]{0,1:T(8,128)(2,1)} %param.24) | copy-start | bytes 786436
  3.2 1.6 %copy-start = (bf16[2048,128]{1,0:T(8,128)(2,1)S(1)}, bf16[2048,128]{1,0:T(8,128)(2,1)}, u32[]{:S(2)}) copy-start(bf16[2048,128]{1,0:T(8,128)(2,1)} %wq.1) | copy-start | bytes 1572868
  3.2 1.6 %copy-start.4 = (bf16[256,256]{1,0:T(8,128)(2,1)S(1)}, bf16[256,256]{1,0:T(8,128)(2,1)}, u32[]{:S(2)}) copy-start(bf16[256,256]{1,0:T(8,128)(2,1)} %act.1) | copy-start | bytes 393220
  3.2 1.6 %copy-start.5 = (f32[256,128]{1,0:T(8,128)S(1)}, f32[256,128]{1,0:T(8,128)}, u32[]{:S(2)}) copy-start(f32[256,128]{1,0:T(8,128)} %constant.5.clone.tb) | copy-start | bytes 393220
  3.3 1.6 %copy-start.6 = (bf16[128,128]{1,0:T(8,128)(2,1)S(1)}, bf16[128,128]{1,0:T(8,128)(2,1)}, u32[]{:S(2)}) copy-start(bf16[128,128]{1,0:T(8,128)(2,1)} %kup.1) | copy-start | bytes 98308
  3.3 1.6 %copy-start.7 = (bf16[128,128]{1,0:T(8,128)(2,1)S(1)}, bf16[128,128]{1,0:T(8,128)(2,1)}, u32[]{:S(2)}) copy-start(bf16[128,128]{1,0:T(8,128)(2,1)} %vup.1) | copy-start | bytes 98308
  3.3 1.6 %copy-start.8 = (f32[64,128]{1,0:T(8,128)S(1)}, f32[64,128]{1,0:T(8,128)}, u32[]{:S(2)}) copy-start(f32[64,128]{1,0:T(8,128)} %constant.4.clone.ta) | copy-start | bytes 98308
  3.3 1.6 %copy-start.9 = (f32[2]{0:T(128)S(1)}, f32[2]{0:T(128)}, u32[]{:S(2)}) copy-start(f32[2]{0:T(128)} %sink.1) | copy-start | bytes 28
  3.3 1.6 %copy-start.10 = (f32[128]{0:T(128)S(1)}, f32[128]{0:T(128)}, u32[]{:S(2)}) copy-start(f32[128]{0:T(128)} %param.25) | copy-start | bytes 1540
  4.9 1.0 %copy-start.1 = (bf16[2048,128]{1,0:T(8,128)(2,1)S(1)}, bf16[2048,128]{1,0:T(8,128)(2,1)}, u32[]{:S(2)}) copy-start(bf16[2048,128]{1,0:T(8,128)(2,1)} %wkvd.1) | copy-start | bytes 1572868
  5.9 1.0 %copy-start.2 = (bf16[128,2048]{1,0:T(8,128)(2,1)S(1)}, bf16[128,2048]{1,0:T(8,128)(2,1)}, u32[]{:S(2)}) copy-start(bf16[128,2048]{1,0:T(8,128)(2,1)} %ow.1) | copy-start | bytes 1572868
  7.0 1.0 %copy-start.3 = (bf16[128,2048]{1,0:T(8,128)(2,1)S(1)}, bf16[128,2048]{1,0:T(8,128)(2,1)}, u32[]{:S(2)}) copy-start(bf16[128,2048]{1,0:T(8,128)(2,1)} %ol.1) | copy-start | bytes 1572868

commit v2 on v1

--- a/solution.py
+++ b/solution.py
@@ -55,9 +55,9 @@
     cfg,
     act, gain, wq, wk, wv, sink, wlq, wkvd, wrope, lgain, kup, vup, ow, ol, ta, tb,
     out,
-    actv, gv, lgv, tav, tbv, sinkv, wqv, wkv, wvv, wlqv, kdv, krv, kupv, vupv, wall,
-    kps, kpr, xb, accq, acck, accv, accl, sqv,
-    kbuf, qt, kvb, catt, cat, mst, lst, acc, pos, por, pls, plr, rss, rsr,
+    actv, gv, lgv, tav, tbv, sinkv, wqv, wtv, kdv, krv, kupv, vupv, wall,
+    kps, kpr, xb, accq, acct, sqv,
+    kbuf, qt, kvb, catt, cat, sco, latt, mst, pos, por, pls, plr, rss, rsr,
     lsem, wssem, wrsem, kpssem, kprsem, xssem, xrsem, kzs, kzr, kys, kyr, kds, kdr,
     qss, qrs, hss, hrs, pss, prs, lss, lrs, rs_s, rs_r,
 ):
@@ -74,6 +74,11 @@
     mate = t + 1 - 2 * c
 
     near, fwd_up, fwd_down = z_plan(nz)
+    n_seen = 2 * REACH + 1 if fwd_up else nz
+    mine = pl.ds(pl.multiple_of(c * 128, 128), 128)
+    mine_lat = pl.ds(pl.multiple_of((2 + c) * 128, 128), 128)
+    theirs = pl.ds(pl.multiple_of(other * 128, 128), 128)
+    theirs_lat = pl.ds(pl.multiple_of((2 + other) * 128, 128), 128)
 
     def at_z(dz):
         return lax.rem(z + dz + nz, nz)
@@ -89,22 +94,6 @@
 
     def done(ref, sem):
         pltpu.make_async_copy(ref, ref, sem).wait()
-
-    rows = pl.ds(pl.multiple_of(t * ft, ft), ft)
-    loads = [
-        (act, actv), (gain, gv), (wkvd.at[rows], kdv), (wrope.at[rows], krv),
-        (lgain, lgv), (ta, tav), (tb, tbv),
-        (wq, wqv.at[c]), (wk, wkv.at[c]), (wv, wvv.at[c]), (wlq, wlqv.at[c]),
-        (kup, kupv.at[c]), (vup, vupv.at[c]), (ow, wall.at[c]), (ol, wall.at[2 + c]),
-    ]
-    local = [pltpu.make_async_copy(a, b, lsem.at[i]) for i, (a, b) in enumerate(loads)]
-    for copy in local:
-        copy.start()
-
-    own_sink = jnp.concatenate(
-        [jnp.full((8, 128), sink[0], F32), jnp.full((8, 128), sink[1], F32)], axis=1
-    )
-    sinkv[c] = own_sink
 
     barrier = pltpu.get_barrier_semaphore()
     n_sig = 0
@@ -124,14 +113,34 @@
     side = lax.rem(s + 2 * c - 1 + sp, sp)
     greet(side, mate)
     n_sig += 1
-    for i in range(4):
-        local[i].wait()
+    rows = pl.ds(pl.multiple_of(t * ft, ft), ft)
+    loads = [
+        (act, actv), (wkvd.at[rows], kdv), (wrope.at[:, rows], krv),
+    ] + [(gain.at[pl.ds(k * ft, ft)], gv.at[k]) for k in range(tp)] + [
+        (lgain, lgv), (ta, tav), (tb, tbv),
+        (wq, wqv.at[c]), (wk, wtv.at[c, 0:64]), (wv, wtv.at[c, 64:128]),
+        (wlq, wtv.at[c, 128:320]),
+        (kup, kupv.at[c]), (vup, vupv.at[c]), (ow, wall.at[mine]), (ol, wall.at[mine_lat]),
+    ]
+    local = [pltpu.make_async_copy(a, b, lsem.at[i]) for i, (a, b) in enumerate(loads)]
+    early = 3 + tp
+    for copy in local[:early]:
+        copy.start()
+
+    own_sink = jnp.concatenate(
+        [jnp.full((8, 128), sink[0], F32), jnp.full((8, 128), sink[1], F32)], axis=1
+    )
+    sinkv[c] = own_sink
+
+    for copy in local[:early]:
+        copy.wait()
     xn = actv[...].astype(F32)
     sq0 = jnp.sum(xn * xn, axis=1, keepdims=True)
     xn = (xn * gv[pl.ds(t, 1), :]).astype(BF16)
     kps[...] = jnp.concatenate(
-        [mm(xn, kdv[...]), mm(xn, krv[...]), jnp.broadcast_to(sq0, (tok, D_ROPE))], axis=1
-    ).reshape(tp, sl, 256)
+        [mm(xn, kdv[...]), mm(xn, krv[...], NT), jnp.broadcast_to(sq0, (tok, D_ROPE))],
+        axis=1,
+    ).astype(BF16).reshape(tp, sl, 256)
     kpr[pl.ds(t, 1)] = kps[pl.ds(t, 1)]
     pl.semaphore_wait(barrier, n_sig)
 
@@ -155,14 +164,16 @@
         return 0
 
     lax.fori_loop(0, tp - 1, send_x, 0)
+    for copy in local[early:]:
+        copy.start()
     wsends = [
-        (wq, wqv.at[c]), (wk, wkv.at[c]), (wv, wvv.at[c]), (wlq, wlqv.at[c]),
-        (kup, kupv.at[c]), (vup, vupv.at[c]), (ow, wall.at[c]), (ol, wall.at[2 + c]),
-        (sinkv.at[c], sinkv.at[c]),
+        (wq, wqv.at[c]), (wk, wtv.at[c, 0:64]), (wv, wtv.at[c, 64:128]),
+        (wlq, wtv.at[c, 128:320]), (kup, kupv.at[c]), (vup, vupv.at[c]),
+        (ow, wall.at[mine]), (ol, wall.at[mine_lat]), (sinkv.at[c], sinkv.at[c]),
     ]
     wdone = [
-        wqv.at[other], wkv.at[other], wvv.at[other], wlqv.at[other], kupv.at[other],
-        vupv.at[other], wall.at[other], wall.at[2 + other], sinkv.at[other],
+        wqv.at[other], wtv.at[other, 0:64], wtv.at[other, 64:128], wtv.at[other, 128:320],
+        kupv.at[other], vupv.at[other], wall.at[theirs], wall.at[theirs_lat], sinkv.at[other],
     ]
     wcopies = [
         rc(a, b, wssem.at[i], wrsem.at[i], s, mate) for i, (a, b) in enumerate(wsends)
@@ -170,8 +181,8 @@
     for copy in wcopies:
         copy.start()
 
-    for i in range(4, 7):
-        local[i].wait()
+    for copy in local[early : early + 3]:
+        copy.wait()
     cos_a, sin_a = tav[pl.ds(s, 1), 0:32], tav[pl.ds(s, 1), 32:64]
 
     def angles(start, count):
@@ -185,9 +196,9 @@
         return 0
 
     lax.fori_loop(0, tp - 1, wait_kp, 0)
-    tot = kpr[0]
+    tot = kpr[0].astype(F32)
     for j in range(1, tp):
-        tot = tot + kpr[j]
+        tot = tot + kpr[j].astype(F32)
     comp, rope, sqs = tot[:, :128], tot[:, 128:192], tot[:, 192:193]
     lat = comp * lax.rsqrt(jnp.mean(comp * comp, axis=1, keepdims=True) + EPSILON) * lgv[...]
     kcos, ksin = angles(t * sl, sl)
@@ -209,22 +220,27 @@
             rc(kbuf.at[zs, c, y], kbuf.at[zs, c, y], kys.at[zs, dy - 1], kyr.at[zs],
                z * ny + at_y(dy), t).start()
 
-    def step_a(dz):
-        zs = at_z(dz)
-        if not (isinstance(dz, int) and dz == 0):
-            done(kbuf.at[zs, c, y], kzr.at[zs])
+    def zs_of(j):
+        far = (j + 1) // 2
+        return lax.rem(z + jnp.where(lax.rem(j, 2) == 0, far, nz - far), nz)
+
+    def step_a(j, _):
+        zs = zs_of(j)
+        done(kbuf.at[zs, c, y], kzr.at[zs])
         y_send(zs)
-
-    def step_b(dz):
-        zs = at_z(dz)
+        return 0
+
+    def step_b(j, _):
+        zs = zs_of(j)
         if ny > 1:
             done(kbuf.at[zs, c, pl.ds(0, ny - 1)], kyr.at[zs])
         rc(kbuf.at[zs, c], kbuf.at[zs, c], kds.at[zs], kdr.at[zs], s, mate).start()
-
-    step_a(0)
-
-    for i in range(7, 11):
-        local[i].wait()
+        return 0
+
+    y_send(z)
+
+    for copy in local[early + 3 : early + 7]:
+        copy.wait()
     for i in range(4):
         done(wdone[i], wrsem.at[i])
 
@@ -234,9 +250,10 @@
         xk = (xf * gv[pl.ds(k, 1), :]).astype(BF16)
         kr = pl.ds(pl.multiple_of(k * ft, ft), ft)
         for c2 in range(2):
-            for a, w in ((accq, wqv), (acck, wkv), (accv, wvv), (accl, wlqv)):
-                term = mm(xk, w[c2, kr, :])
-                a[c2] = term if first else a[c2] + term
+            term = mm(xk, wqv[c2, kr, :])
+            accq[c2] = term if first else accq[c2] + term
+            term = mm(xk, wtv[c2, :, kr], NT)
+            acct[c2] = term if first else acct[c2] + term
         sqv[...] = sq if first else sqv[...] + sq
 
     own_half = pl.ds(pl.multiple_of(c * ht, ht), ht)
@@ -248,32 +265,10 @@
         project(xb[k], k, False)
         return 0
 
-    lax.fori_loop(0, tp - 1, project_next, 0)
-
-    scale = lax.rsqrt(sqv[...] / model + EPSILON)
-    local[11].wait()
-    done(wdone[4], wrsem.at[4])
-    qcos, qsin = angles(c * ht, ht)
-    factor = (PLAIN + D_ROPE) ** (-0.5) * LOG2E
-    for c2 in range(2):
-        ql = accl[c2] * scale
-        plain = ql[:, :PLAIN].astype(BF16)
-        qt[x, 0:128, c2 * ht : (c2 + 1) * ht] = (mm(kupv[c2], plain, NT) * factor).astype(BF16)
-        turned = rotate(ql[:, PLAIN:], qcos, qsin) * factor
-        qt[x, 128:192, c2 * ht : (c2 + 1) * ht] = jnp.transpose(turned).astype(BF16)
-    for dx in range(1, nx):
-        xo = lax.rem(x + dx, nx)
-        rc(qt.at[x], qt.at[x], qss.at[dx - 1], qrs.at[x], s, xo * 2 + c).start()
-
-    for c2 in range(2):
-        kvb[1, c2, :, 0:64] = (acck[c2] * scale).astype(BF16)
-        kvb[1, c2, :, 64:128] = (accv[c2] * scale).astype(BF16)
-    to_mate = rc(kvb.at[1], kvb.at[2 * c], hss.at[0], hrs.at[2 * c], s, mate)
-    to_mate.start()
-    to_side = rc(kvb.at[1], kvb.at[2 * other], hss.at[1], hrs.at[2 * other], side, mate)
-    to_side.start()
+    lax.fori_loop(0, tp - 3, project_next, 0)
 
     if fwd_up:
+        lax.fori_loop(1, 2 * REACH - 1, step_a, 0)
         zs = at_z(-REACH)
         done(kbuf.at[zs, c, y], kzr.at[zs])
         for i, dz in enumerate(fwd_up):
@@ -284,16 +279,36 @@
         for i, dz in enumerate(fwd_down):
             z_send(dz, zs, len(near) + len(fwd_up) + i)
         y_send(zs)
-        first = [dz for dz in near if abs(dz) != REACH]
-        late = [-(REACH + k) for k in fwd_up[::-1]] + [REACH - k for k in fwd_down[::-1]]
-        late.sort(key=abs)
-        seen = [0] + first + [-REACH, REACH]
     else:
-        first, late, seen = [-dz for dz in near], [], [0] + [-dz for dz in near]
-    for dz in first:
-        step_a(dz)
-    for dz in seen:
-        step_b(dz)
+        lax.fori_loop(1, nz, step_a, 0)
+    lax.fori_loop(max(tp - 3, 0), tp - 1, project_next, 0)
+
+    scale = lax.rsqrt(sqv[...] / model + EPSILON)
+    local[early + 7].wait()
+    done(wdone[4], wrsem.at[4])
+    qcos, qsin = angles(c * ht, ht)
+    factor = (PLAIN + D_ROPE) ** (-0.5) * LOG2E
+    for c2 in range(2):
+        ql = acct[c2, :, 128:320] * scale
+        plain = ql[:, :PLAIN].astype(BF16)
+        qt[x, 0:128, c2 * ht : (c2 + 1) * ht] = (mm(kupv[c2], plain, NT) * factor).astype(BF16)
+        turned = rotate(ql[:, PLAIN:], qcos, qsin) * factor
+        qt[x, 128:192, c2 * ht : (c2 + 1) * ht] = jnp.transpose(turned).astype(BF16)
+    for dx in range(1, nx):
+        xo = lax.rem(x + dx, nx)
+        rc(qt.at[x], qt.at[x], qss.at[dx - 1], qrs.at[x], s, xo * 2 + c).start()
+
+    for c2 in range(2):
+        kvb[1, c2] = (acct[c2, :, 0:128] * scale).astype(BF16)
+    to_mate = rc(kvb.at[1], kvb.at[2 * c], hss.at[0], hrs.at[2 * c], s, mate)
+    to_mate.start()
+    to_side = rc(kvb.at[1], kvb.at[2 * other], hss.at[1], hrs.at[2 * other], side, mate)
+    to_side.start()
+
+    early_b = min(5, n_seen)
+    lax.fori_loop(0, early_b, step_b, 0)
+    lax.fori_loop(n_seen, nz, step_a, 0)
+    lax.fori_loop(early_b, n_seen, step_b, 0)
 
     for i in (0, 2):
         done(kvb.at[i], hrs.at[i])
@@ -322,55 +337,67 @@
             o = mm(vw, w.astype(BF16), TN) / den
             catt[(c2 * 2 + g) * DH : (c2 * 2 + g + 1) * DH, :] = o.astype(BF16)
 
-    for dz in late:
-        step_a(dz)
-    for dz in late:
-        step_b(dz)
-
     for dx in range(1, nx):
         xo = lax.rem(x + dx, nx)
         done(qt.at[xo], qrs.at[xo])
     mst[...] = jnp.full(mst.shape, -jnp.inf, F32)
-    lst[...] = jnp.zeros(lst.shape, F32)
-    acc[...] = jnp.zeros(acc.shape, F32)
     nkeys = 2 * ny * sl
-
-    def batch(j, _):
-        near_j = (j + 1) // 2
-        dz = jnp.where(lax.rem(j, 2) == 0, near_j, -near_j)
-        zs = lax.rem(z + dz + nz, nz)
+    keys_all = nz * nkeys
+
+    def step_c(j, _):
+        zs = zs_of(j)
         done(kbuf.at[zs, other], kdr.at[zs])
         both = kbuf[zs].reshape(2 * ny, sl + sl // 2, 128)
         latk = both[:, :sl, :].reshape(nkeys, 128)
         rp = both[:, sl:, :]
         rk = jnp.concatenate([rp[:, :, 0:64], rp[:, :, 64:128]], axis=1).reshape(nkeys, 64)
         keys = jnp.concatenate([latk, rk], axis=1)
-        latt = jnp.transpose(latk)
+        at = pl.ds(pl.multiple_of(zs * nkeys, nkeys), nkeys)
+        latt[:, at] = jnp.transpose(latk)
         for xp in range(nx):
             sc = mm(keys, qt[xp])
-            m_old = mst[xp]
-            m_new = jnp.maximum(m_old, jnp.max(sc, axis=0, keepdims=True))
-            alpha = jnp.exp2(m_old - m_new)
-            p = jnp.exp2(sc - m_new)
-            mst[xp] = m_new
-            lst[xp] = lst[xp] * alpha + jnp.sum(p, axis=0, keepdims=True)
-            acc[xp] = acc[xp] * alpha + mm(latt, p.astype(BF16))
-        return 0
-
-    lax.fori_loop(0, nz, batch, 0)
-
-    for xp in range(nx):
-        l = lst[xp]
-        pos[xp] = (acc[xp] / l).astype(BF16)
-        pls[xp] = jnp.broadcast_to(mst[xp] + jnp.log(l) * LOG2E, (8, 2 * ht))
-    for dx in range(1, nx):
+            sco[xp, at, :] = sc
+            mst[xp] = jnp.maximum(mst[xp], jnp.max(sc.reshape(nkeys // 8, 8, 2 * ht), axis=0))
+        return 0
+
+    def step_cb(i, _):
+        step_c(i, 0)
+        step_b(n_seen + i, 0)
+        return 0
+
+    lax.fori_loop(0, nz - n_seen, step_cb, 0)
+    lax.fori_loop(nz - n_seen, nz, step_c, 0)
+
+    part = min(1024, keys_all)
+
+    def weigh(xp):
+        peak = jnp.max(mst[xp], axis=0, keepdims=True)
+        l8 = jnp.zeros((8, 2 * ht), F32)
+        o = jnp.zeros((128, 2 * ht), F32)
+        for k in range(keys_all // part):
+            p = jnp.exp2(sco[xp, k * part : (k + 1) * part, :] - peak)
+            l8 = l8 + jnp.sum(p.reshape(part // 8, 8, 2 * ht), axis=0)
+            o = o + mm(latt[:, k * part : (k + 1) * part], p.astype(BF16))
+        l = jnp.sum(l8, axis=0, keepdims=True)
+        pos[xp] = (o / l).astype(BF16)
+        pls[xp] = jnp.broadcast_to(peak + jnp.log(l) * LOG2E, (8, 2 * ht))
+
+    def weigh_next(i, _):
+        dx = i + 1
+        if nx == 4:
+            dx = jnp.where(dx == 3, 3, 3 - dx)
         xo = lax.rem(x + dx, nx)
-        rc(pls.at[xo], plr.at[x], lss.at[dx - 1], lrs.at[x], s, xo * 2 + c).start()
-        rc(pos.at[xo], por.at[x], pss.at[dx - 1], prs.at[x], s, xo * 2 + c).start()
+        weigh(xo)
+        rc(pls.at[xo], plr.at[x], lss.at[i], lrs.at[x], s, xo * 2 + c).start()
+        rc(pos.at[xo], por.at[x], pss.at[i], prs.at[x], s, xo * 2 + c).start()
+        return 0
+
+    lax.fori_loop(0, nx - 1, weigh_next, 0)
+    weigh(x)
     por[pl.ds(x, 1)] = pos[pl.ds(x, 1)]
     plr[pl.ds(x, 1)] = pls[pl.ds(x, 1)]
-    for i in range(12, 15):
-        local[i].wait()
+    for copy in local[early + 8 :]:
+        copy.wait()
     for i in range(5, 8):
         done(wdone[i], wrsem.at[i])
     for dx in range(1, nx):
@@ -391,26 +418,18 @@
         ).astype(BF16)
     cat[...] = jnp.transpose(catt[...])
 
-    def out_block(d, _):
+    def out_block(j):
+        cols = pl.ds(pl.multiple_of(j * ft, ft), ft)
+        return mm(cat[...], wall[:, cols]).astype(BF16)
+
+    def send_block(d, _):
         j = order(d)
-        cols = pl.ds(pl.multiple_of(j * ft, ft), ft)
-        o = mm(cat[:, 0:128], wall[0, :, cols])
-        for i in range(1, 4):
-            o = o + mm(cat[:, i * 128 : (i + 1) * 128], wall[i, :, cols])
-        rss[j] = o.astype(BF16)
-        return j
-
-    def send_block(d, _):
-        j = out_block(d, _)
+        rss[j] = out_block(j)
         rc(rss.at[j], rsr.at[x, c], rs_s.at[d], rs_r.at[x, c], s, j).start()
         return 0
 
     lax.fori_loop(0, tp - 1, send_block, 0)
-    cols = pl.ds(pl.multiple_of(t * ft, ft), ft)
-    o = mm(cat[:, 0:128], wall[0, :, cols])
-    for i in range(1, 4):
-        o = o + mm(cat[:, i * 128 : (i + 1) * 128], wall[i, :, cols])
-    rsr[x, c] = o.astype(BF16)
+    rsr[x, c] = out_block(t)
 
     def wait_block(d, _):
         j = order(tp - 2 - d)
@@ -480,19 +499,18 @@
     scratch = [
         v((tok, ft), BF16), v((tp, ft), F32), v((1, 128), F32), v((sp, 128), F32),
         v((tok, 128), F32), v((2, 8, 256), F32), v((2, model, 128), BF16),
-        v((2, model, 64), BF16), v((2, model, 64), BF16), v((2, model, 192), BF16),
-        v((ft, 128), BF16), v((ft, 64), BF16), v((2, 128, 128), BF16), v((2, 128, 128), BF16),
-        v((4, 128, model), BF16),
-        v((tp, sl, 256), F32), v((tp, sl, 256), F32), v((tp, ht, ft), BF16),
-        v((2, ht, 128), F32), v((2, ht, 64), F32), v((2, ht, 64), F32), v((2, ht, 192), F32),
-        v((ht, 1), F32),
+        v((2, 320, model), BF16), v((ft, 128), BF16), v((64, ft), BF16),
+        v((2, 128, 128), BF16), v((2, 128, 128), BF16), v((512, model), BF16),
+        v((tp, sl, 256), BF16), v((tp, sl, 256), BF16), v((tp, ht, ft), BF16),
+        v((2, ht, 128), F32), v((2, ht, 320), F32), v((ht, 1), F32),
         v((nz, 2, ny, sl + sl // 2, 128), BF16), v((nx, 192, 2 * ht), BF16),
         v((3, 2, ht, 128), BF16), v((512, ht), BF16), v((ht, 512), BF16),
-        v((nx, 1, 2 * ht), F32), v((nx, 1, 2 * ht), F32), v((nx, 128, 2 * ht), F32),
+        v((nx, tok * sp // nx, 2 * ht), F32), v((128, tok * sp // nx), BF16),
+        v((nx, 8, 2 * ht), F32),
         v((nx, 128, 2 * ht), BF16), v((nx, 128, 2 * ht), BF16),
         v((nx, 8, 2 * ht), F32), v((nx, 8, 2 * ht), F32),
         v((tp, ht, ft), BF16), v((nx, 2, ht, ft), BF16),
-        dma((15,)), dma((9,)), dma((9,)), dma((tp,)), dma((tp,)), dma((tp,)), dma((tp,)),
+        dma((14 + tp,)), dma((9,)), dma((9,)), dma((tp,)), dma((tp,)), dma((tp,)), dma((tp,)),
         dma((n_z,)), dma((nz,)), dma((nz, max(ny - 1, 1))), dma((nz,)), dma((nz,)), dma((nz,)),
         dma((nx,)), dma((nx,)), dma((2,)), dma((3,)), dma((nx,)), dma((nx,)), dma((nx,)), dma((nx,)),
         dma((tp,)), dma((nx, 2)),
@@ -507,11 +525,10 @@
         out_specs=pl.BlockSpec(memory_space=pltpu.VMEM),
         scratch_shapes=scratch,
         compiler_params=pltpu.CompilerParams(
-            collective_id=0, has_side_effects=True, vmem_limit_bytes=48 * 1024 * 1024
+            collective_id=0, has_side_effects=True, vmem_limit_bytes=67043328
         ),
     )(
-        act, gain.reshape(tp, ft), wq, wk, wv, sink, wlq, wkvd, wrope,
-        lgain.reshape(1, 128), kup, vup, ow, ol, jnp.asarray(ta), jnp.asarray(tb),
+        act, gain, wq, wk.T, wv.T, sink, wlq.T, wkvd, wrope.T, lgain.reshape(1, 128), kup, vup, ow, ol, jnp.asarray(ta), jnp.asarray(tb),
     )
 
 

time: 87.2 us -> 59.7 us (0.68)
  Pallas kernels: 77.7 us -> 57.9 us
  local copies, waits for them, and re-layouts: 8.5 us -> 1.57 us
    pallas_call x1, Pallas kernels: 77.7 us -> 57.9 us  [per_device(): pl.pallas_call(functools.partial(kernel, cfg), out_shape=jax.ShapeDtypeSt...]
    unnamed x31 -> x1, local copies, waits for them, and re-layouts: 7.8 us -> 1.57 us
where the time goes in v2:
time: 59.7 us; the launch traced here: 59.5 us
  Pallas kernels  57.9 us (97%)
  local copies, waits for them, and re-layouts  1.57 us (3%)
    pallas_call x1, Pallas kernels, per_device(): pl.pallas_call(functools.partial(kernel, cfg), out_shape=jax.ShapeDtypeSt...  57.9 us
    unnamed x1, local copies, waits for them, and re-layouts  1.57 us

profile of v2, /device:TPU:1, one launch (start us, length us, event | category | flops | bytes accessed | tf_op | source)
XLA Modules:
  0.0 59.5 jit_solution(566176282571773518)
XLA Ops:
  0.0 57.9 %shard_map.154 = bf16[256,256]{1,0:T(8,128)(2,1)} custom-call(bf16[256,256]{1,0:T(8,128)(2,1)} %act.1, f32[2048]{0:T(1024)} %gain.1, bf16[2048,128]{1,0:T(8,128)(2,1)} %wq.1, bf16[64,2048]{1,0:T(8,128)(2,1)} %bitcast.6, bf16[64,2048]{1,0:T(8,128)(2,1)} %bitcast.7, f32[2]{0:T(128)} %sink.1, bf16[192,2048]{1,0:T(8,128)(2,1)} %bitcast.5, ...), custom_call_target="tpu_custom_call" | custom-call | tf_op jit(solution)/shard_map/pallas_call | solution.py:521
  57.9 1.6 %copy.18 = bf16[256,256]{1,0:T(8,128)(2,1)} copy(bf16[256,256]{1,0:T(8,128)(2,1)} %shard_map.154) | data formatting | bytes 262144

commit v3 on v2

--- a/solution.py
+++ b/solution.py
@@ -31,11 +31,12 @@
 
 
 def z_plan(nz):
-    if nz == 4 * REACH:
+    if nz > 2 * REACH:
         near = [REACH, -REACH]
         for k in range(1, REACH):
             near += [k, -k]
-        return near, list(range(1, REACH + 1))[::-1], [-k for k in range(1, REACH)][::-1]
+        rest = nz // 2 - REACH
+        return near, list(range(1, rest + 1))[::-1], [-k for k in range(1, rest)][::-1]
     half = nz // 2
     near = []
     for k in range(1, half + 1):
@@ -57,7 +58,7 @@
     out,
     actv, gv, lgv, tav, tbv, sinkv, wqv, wtv, kdv, krv, kupv, vupv, wall,
     kps, kpr, xb, accq, acct, sqv,
-    kbuf, qt, kvb, catt, cat, sco, latt, mst, pos, por, pls, plr, rss, rsr,
+    kbuf, qt, kvb, catt, cat, sco, latt, keyb, mst, pos, por, pls, plr, rss, rsr,
     lsem, wssem, wrsem, kpssem, kprsem, xssem, xrsem, kzs, kzr, kys, kyr, kds, kdr,
     qss, qrs, hss, hrs, pss, prs, lss, lrs, rs_s, rs_r,
 ):
@@ -150,6 +151,12 @@
             hop = jnp.where(hop == 3, 3, 3 - hop)
         return jnp.where(d < tp - 2, lax.rem((x + hop) * 2 + lax.rem(c + d, 2), tp), mate)
 
+    def order_x(d):
+        hop = d // 2 + 1
+        if nx == 4:
+            hop = jnp.where(hop == 1, 1, 5 - hop)
+        return jnp.where(d < tp - 2, lax.rem((x + hop) * 2 + lax.rem(c + d, 2), tp), mate)
+
     def send_kp(d, _):
         j = order(d)
         rc(kps.at[j], kpr.at[t], kpssem.at[d], kprsem.at[t], s, j).start()
@@ -158,7 +165,7 @@
     lax.fori_loop(0, tp - 1, send_kp, 0)
 
     def send_x(d, _):
-        j = order(d)
+        j = order_x(d)
         half = pl.ds(pl.multiple_of(lax.rem(j, 2) * ht, ht), ht)
         rc(actv.at[half], xb.at[t], xssem.at[d], xrsem.at[t], s, j).start()
         return 0
@@ -260,7 +267,7 @@
     project(actv[own_half, :], t, True)
 
     def project_next(d, _):
-        k = order(tp - 2 - d)
+        k = order_x(lax.rem(d + tp - 2, tp - 1))
         done(xb.at[k], xrsem.at[k])
         project(xb[k], k, False)
         return 0
@@ -268,7 +275,7 @@
     lax.fori_loop(0, tp - 3, project_next, 0)
 
     if fwd_up:
-        lax.fori_loop(1, 2 * REACH - 1, step_a, 0)
+        lax.fori_loop(1, n_seen - 2, step_a, 0)
         zs = at_z(-REACH)
         done(kbuf.at[zs, c, y], kzr.at[zs])
         for i, dz in enumerate(fwd_up):
@@ -294,9 +301,11 @@
         qt[x, 0:128, c2 * ht : (c2 + 1) * ht] = (mm(kupv[c2], plain, NT) * factor).astype(BF16)
         turned = rotate(ql[:, PLAIN:], qcos, qsin) * factor
         qt[x, 128:192, c2 * ht : (c2 + 1) * ht] = jnp.transpose(turned).astype(BF16)
-    for dx in range(1, nx):
+    sides = [1, 3] if nx == 4 else list(range(1, nx))
+    across = [2] if nx == 4 else []
+    for i, dx in enumerate(sides + across):
         xo = lax.rem(x + dx, nx)
-        rc(qt.at[x], qt.at[x], qss.at[dx - 1], qrs.at[x], s, xo * 2 + c).start()
+        rc(qt.at[x], qt.at[x], qss.at[i], qrs.at[x], s, xo * 2 + c).start()
 
     for c2 in range(2):
         kvb[1, c2] = (acct[c2, :, 0:128] * scale).astype(BF16)
@@ -305,10 +314,60 @@
     to_side = rc(kvb.at[1], kvb.at[2 * other], hss.at[1], hrs.at[2 * other], side, mate)
     to_side.start()
 
-    early_b = min(5, n_seen)
+    mst[...] = jnp.full(mst.shape, -jnp.inf, F32)
+    nkeys = 2 * ny * sl
+    keys_all = nz * nkeys
+
+    def prep(i, _):
+        for u in range(2):
+            j = 2 * i + u
+            zs = zs_of(j)
+            done(kbuf.at[zs, other], kdr.at[zs])
+            both = kbuf[zs].reshape(2 * ny, sl + sl // 2, 128)
+            latk = both[:, :sl, :].reshape(nkeys, 128)
+            rp = both[:, sl:, :]
+            rk = jnp.concatenate([rp[:, :, 0:64], rp[:, :, 64:128]], axis=1)
+            at = pl.ds(pl.multiple_of(j * nkeys, nkeys), nkeys)
+            keyb[at, 0:128] = latk
+            keyb[at, 128:192] = rk.reshape(nkeys, 64)
+            latt[:, at] = jnp.transpose(latk)
+        score(i, x)
+        return 0
+
+    def score(i, xp):
+        at = pl.ds(pl.multiple_of(i * 2 * nkeys, 2 * nkeys), 2 * nkeys)
+        sc = mm(keyb[at, :], qt[xp])
+        sco[xp, at, :] = sc
+        mst[xp] = jnp.maximum(mst[xp], jnp.max(sc.reshape(nkeys // 4, 8, 2 * ht), axis=0))
+
+    def score_sides(i, _):
+        for dx in sides:
+            score(i, lax.rem(x + dx, nx))
+        return 0
+
+    def score_across(i, _):
+        for dx in across:
+            score(i, lax.rem(x + dx, nx))
+        return 0
+
+    def score_all(i, _):
+        prep(i, 0)
+        score_sides(i, 0)
+        return score_across(i, 0)
+
+    def wait_queries(dxs):
+        for dx in dxs:
+            xo = lax.rem(x + dx, nx)
+            done(qt.at[xo], qrs.at[xo])
+
+    pairs = nz // 2
+    seen_p = n_seen // 2
+    early_b, early_p, mid_p = min(5, n_seen), min(1, seen_p), min(2, seen_p)
     lax.fori_loop(0, early_b, step_b, 0)
+    lax.fori_loop(0, early_p, prep, 0)
     lax.fori_loop(n_seen, nz, step_a, 0)
     lax.fori_loop(early_b, n_seen, step_b, 0)
+    lax.fori_loop(early_p, mid_p, prep, 0)
 
     for i in (0, 2):
         done(kvb.at[i], hrs.at[i])
@@ -337,38 +396,30 @@
             o = mm(vw, w.astype(BF16), TN) / den
             catt[(c2 * 2 + g) * DH : (c2 * 2 + g + 1) * DH, :] = o.astype(BF16)
 
-    for dx in range(1, nx):
-        xo = lax.rem(x + dx, nx)
-        done(qt.at[xo], qrs.at[xo])
-    mst[...] = jnp.full(mst.shape, -jnp.inf, F32)
-    nkeys = 2 * ny * sl
-    keys_all = nz * nkeys
-
-    def step_c(j, _):
-        zs = zs_of(j)
-        done(kbuf.at[zs, other], kdr.at[zs])
-        both = kbuf[zs].reshape(2 * ny, sl + sl // 2, 128)
-        latk = both[:, :sl, :].reshape(nkeys, 128)
-        rp = both[:, sl:, :]
-        rk = jnp.concatenate([rp[:, :, 0:64], rp[:, :, 64:128]], axis=1).reshape(nkeys, 64)
-        keys = jnp.concatenate([latk, rk], axis=1)
-        at = pl.ds(pl.multiple_of(zs * nkeys, nkeys), nkeys)
-        latt[:, at] = jnp.transpose(latk)
-        for xp in range(nx):
-            sc = mm(keys, qt[xp])
-            sco[xp, at, :] = sc
-            mst[xp] = jnp.maximum(mst[xp], jnp.max(sc.reshape(nkeys // 8, 8, 2 * ht), axis=0))
-        return 0
-
-    def step_cb(i, _):
-        step_c(i, 0)
-        step_b(n_seen + i, 0)
-        return 0
-
-    lax.fori_loop(0, nz - n_seen, step_cb, 0)
-    lax.fori_loop(nz - n_seen, nz, step_c, 0)
-
-    part = min(1024, keys_all)
+    lax.fori_loop(mid_p, seen_p, prep, 0)
+    wait_queries(sides)
+    n_two = seen_p // 2
+    rest = nz - n_seen - 2 * n_two
+
+    def sides_b(i, _):
+        for u in range(2):
+            score_sides(2 * i + u, 0)
+        for u in range(2 if rest >= 0 else 0):
+            step_b(n_seen + 2 * i + u, 0)
+        return 0
+
+    def b_all(i, _):
+        step_b(n_seen + 2 * n_two + i, 0)
+        return score_all(seen_p + i, 0)
+
+    lax.fori_loop(0, n_two, sides_b, 0)
+    lax.fori_loop(2 * n_two, seen_p, score_sides, 0)
+    wait_queries(across)
+    lax.fori_loop(0, seen_p, score_across, 0)
+    lax.fori_loop(0, max(rest, 0), b_all, 0)
+    lax.fori_loop(seen_p + max(rest, 0), pairs, score_all, 0)
+
+    part = min(512, keys_all)
 
     def weigh(xp):
         peak = jnp.max(mst[xp], axis=0, keepdims=True)
@@ -506,6 +557,7 @@
         v((nz, 2, ny, sl + sl // 2, 128), BF16), v((nx, 192, 2 * ht), BF16),
         v((3, 2, ht, 128), BF16), v((512, ht), BF16), v((ht, 512), BF16),
         v((nx, tok * sp // nx, 2 * ht), F32), v((128, tok * sp // nx), BF16),
+        v((tok * sp // nx, 192), BF16),
         v((nx, 8, 2 * ht), F32),
         v((nx, 128, 2 * ht), BF16), v((nx, 128, 2 * ht), BF16),
         v((nx, 8, 2 * ht), F32), v((nx, 8, 2 * ht), F32),

time: 59.7 us -> 59 us (0.988)
  Pallas kernels: 57.9 us -> 57.2 us
    pallas_call x1, Pallas kernels: 57.9 us -> 57.2 us  [per_device(): pl.pallas_call(functools.partial(kernel, cfg), out_shape=jax.ShapeDtypeSt...]
where the time goes in v3:
time: 59 us; the launch traced here: 58.8 us
  Pallas kernels  57.2 us (97%)
  local copies, waits for them, and re-layouts  1.57 us (3%)
    pallas_call x1, Pallas kernels, per_device(): pl.pallas_call(functools.partial(kernel, cfg), out_shape=jax.ShapeDtypeSt...  57.2 us
    unnamed x1, local copies, waits for them, and re-layouts  1.57 us

profile of v3, /device:TPU:1, one launch (start us, length us, event | category | flops | bytes accessed | tf_op | source)
XLA Modules:
  0.0 58.8 jit_solution(11028007434860898252)
XLA Ops:
  0.0 57.2 %shard_map.154 = bf16[256,256]{1,0:T(8,128)(2,1)} custom-call(bf16[256,256]{1,0:T(8,128)(2,1)} %act.1, f32[2048]{0:T(1024)} %gain.1, bf16[2048,128]{1,0:T(8,128)(2,1)} %wq.1, bf16[64,2048]{1,0:T(8,128)(2,1)} %bitcast.6, bf16[64,2048]{1,0:T(8,128)(2,1)} %bitcast.7, f32[2]{0:T(128)} %sink.1, bf16[192,2048]{1,0:T(8,128)(2,1)} %bitcast.5, ...), custom_call_target="tpu_custom_call" | custom-call | tf_op jit(solution)/shard_map/pallas_call | solution.py:573
  57.2 1.6 %copy.18 = bf16[256,256]{1,0:T(8,128)(2,1)} copy(bf16[256,256]{1,0:T(8,128)(2,1)} %shard_map.154) | data formatting | bytes 262144

commit v4 on v3

--- a/solution.py
+++ b/solution.py
@@ -56,7 +56,7 @@
     cfg,
     act, gain, wq, wk, wv, sink, wlq, wkvd, wrope, lgain, kup, vup, ow, ol, ta, tb,
     out,
-    actv, gv, lgv, tav, tbv, sinkv, wqv, wtv, kdv, krv, kupv, vupv, wall,
+    actv, gv, lgv, tav, tbv, sinkm, sinkv, wqv, wtv, kdv, krv, kupv, vupv, wall,
     kps, kpr, xb, accq, acct, sqv,
     kbuf, qt, kvb, catt, cat, sco, latt, keyb, mst, pos, por, pls, plr, rss, rsr,
     lsem, wssem, wrsem, kpssem, kprsem, xssem, xrsem, kzs, kzr, kys, kyr, kds, kdr,
@@ -116,7 +116,7 @@
     n_sig += 1
     rows = pl.ds(pl.multiple_of(t * ft, ft), ft)
     loads = [
-        (act, actv), (wkvd.at[rows], kdv), (wrope.at[:, rows], krv),
+        (act, actv), (sink, sinkm), (wkvd.at[rows], kdv), (wrope.at[:, rows], krv),
     ] + [(gain.at[pl.ds(k * ft, ft)], gv.at[k]) for k in range(tp)] + [
         (lgain, lgv), (ta, tav), (tb, tbv),
         (wq, wqv.at[c]), (wk, wtv.at[c, 0:64]), (wv, wtv.at[c, 64:128]),
@@ -124,17 +124,17 @@
         (kup, kupv.at[c]), (vup, vupv.at[c]), (ow, wall.at[mine]), (ol, wall.at[mine_lat]),
     ]
     local = [pltpu.make_async_copy(a, b, lsem.at[i]) for i, (a, b) in enumerate(loads)]
-    early = 3 + tp
+    early = 4 + tp
     for copy in local[:early]:
         copy.start()
 
+    for copy in local[:early]:
+        copy.wait()
     own_sink = jnp.concatenate(
-        [jnp.full((8, 128), sink[0], F32), jnp.full((8, 128), sink[1], F32)], axis=1
+        [jnp.full((8, 128), sinkm[0], F32), jnp.full((8, 128), sinkm[1], F32)], axis=1
     )
     sinkv[c] = own_sink
 
-    for copy in local[:early]:
-        copy.wait()
     xn = actv[...].astype(F32)
     sq0 = jnp.sum(xn * xn, axis=1, keepdims=True)
     xn = (xn * gv[pl.ds(t, 1), :]).astype(BF16)
@@ -274,8 +274,13 @@
 
     lax.fori_loop(0, tp - 3, project_next, 0)
 
+    first_a = min(3, n_seen - 2) if fwd_up else nz
+    first_b = min(3, n_seen)
+    lax.fori_loop(1, first_a, step_a, 0)
+    step_b(0, 0)
+    lax.fori_loop(max(tp - 3, 0), tp - 1, project_next, 0)
     if fwd_up:
-        lax.fori_loop(1, n_seen - 2, step_a, 0)
+        lax.fori_loop(first_a, n_seen - 2, step_a, 0)
         zs = at_z(-REACH)
         done(kbuf.at[zs, c, y], kzr.at[zs])
         for i, dz in enumerate(fwd_up):
@@ -286,9 +291,6 @@
         for i, dz in enumerate(fwd_down):
             z_send(dz, zs, len(near) + len(fwd_up) + i)
         y_send(zs)
-    else:
-        lax.fori_loop(1, nz, step_a, 0)
-    lax.fori_loop(max(tp - 3, 0), tp - 1, project_next, 0)
 
     scale = lax.rsqrt(sqv[...] / model + EPSILON)
     local[early + 7].wait()
@@ -298,14 +300,14 @@
     for c2 in range(2):
         ql = acct[c2, :, 128:320] * scale
         plain = ql[:, :PLAIN].astype(BF16)
-        qt[x, 0:128, c2 * ht : (c2 + 1) * ht] = (mm(kupv[c2], plain, NT) * factor).astype(BF16)
+        qt[0, 0:128, c2 * ht : (c2 + 1) * ht] = (mm(kupv[c2], plain, NT) * factor).astype(BF16)
         turned = rotate(ql[:, PLAIN:], qcos, qsin) * factor
-        qt[x, 128:192, c2 * ht : (c2 + 1) * ht] = jnp.transpose(turned).astype(BF16)
+        qt[0, 128:192, c2 * ht : (c2 + 1) * ht] = jnp.transpose(turned).astype(BF16)
     sides = [1, 3] if nx == 4 else list(range(1, nx))
     across = [2] if nx == 4 else []
     for i, dx in enumerate(sides + across):
         xo = lax.rem(x + dx, nx)
-        rc(qt.at[x], qt.at[x], qss.at[i], qrs.at[x], s, xo * 2 + c).start()
+        rc(qt.at[0], qt.at[nx - dx], qss.at[i], qrs.at[nx - dx], s, xo * 2 + c).start()
 
     for c2 in range(2):
         kvb[1, c2] = (acct[c2, :, 0:128] * scale).astype(BF16)
@@ -318,7 +320,10 @@
     nkeys = 2 * ny * sl
     keys_all = nz * nkeys
 
-    def prep(i, _):
+    def pair(i):
+        return pl.ds(pl.multiple_of(i * 2 * nkeys, 2 * nkeys), 2 * nkeys)
+
+    def take(i):
         for u in range(2):
             j = 2 * i + u
             zs = zs_of(j)
@@ -331,40 +336,38 @@
             keyb[at, 0:128] = latk
             keyb[at, 128:192] = rk.reshape(nkeys, 64)
             latt[:, at] = jnp.transpose(latk)
-        score(i, x)
-        return 0
-
-    def score(i, xp):
-        at = pl.ds(pl.multiple_of(i * 2 * nkeys, 2 * nkeys), 2 * nkeys)
-        sc = mm(keyb[at, :], qt[xp])
-        sco[xp, at, :] = sc
-        mst[xp] = jnp.maximum(mst[xp], jnp.max(sc.reshape(nkeys // 4, 8, 2 * ht), axis=0))
-
-    def score_sides(i, _):
-        for dx in sides:
-            score(i, lax.rem(x + dx, nx))
-        return 0
-
-    def score_across(i, _):
-        for dx in across:
-            score(i, lax.rem(x + dx, nx))
-        return 0
-
-    def score_all(i, _):
-        prep(i, 0)
-        score_sides(i, 0)
-        return score_across(i, 0)
+
+    def score(i, dx):
+        sc = mm(keyb[pair(i), :], qt[dx])
+        sco[dx, pair(i), :] = sc
+        mst[dx] = jnp.maximum(mst[dx], jnp.max(sc.reshape(nkeys // 4, 8, 2 * ht), axis=0))
+
+    def prep(i, _):
+        take(i)
+        score(i, 0)
+        return 0
+
+    def rest_of(i, _):
+        for dx in across + sides:
+            score(i, dx)
+        return 0
+
+    def all_of(i, _):
+        take(i)
+        for dx in across + sides + [0]:
+            score(i, dx)
+        return 0
 
     def wait_queries(dxs):
         for dx in dxs:
-            xo = lax.rem(x + dx, nx)
-            done(qt.at[xo], qrs.at[xo])
+            done(qt.at[dx], qrs.at[dx])
 
     pairs = nz // 2
     seen_p = n_seen // 2
     early_b, early_p, mid_p = min(5, n_seen), min(1, seen_p), min(2, seen_p)
-    lax.fori_loop(0, early_b, step_b, 0)
+    lax.fori_loop(1, first_b, step_b, 0)
     lax.fori_loop(0, early_p, prep, 0)
+    lax.fori_loop(first_b, early_b, step_b, 0)
     lax.fori_loop(n_seen, nz, step_a, 0)
     lax.fori_loop(early_b, n_seen, step_b, 0)
     lax.fori_loop(early_p, mid_p, prep, 0)
@@ -397,64 +400,52 @@
             catt[(c2 * 2 + g) * DH : (c2 * 2 + g + 1) * DH, :] = o.astype(BF16)
 
     lax.fori_loop(mid_p, seen_p, prep, 0)
-    wait_queries(sides)
+    wait_queries(sides + across)
     n_two = seen_p // 2
     rest = nz - n_seen - 2 * n_two
 
-    def sides_b(i, _):
+    def rest_b(i, _):
         for u in range(2):
-            score_sides(2 * i + u, 0)
+            rest_of(2 * i + u, 0)
         for u in range(2 if rest >= 0 else 0):
             step_b(n_seen + 2 * i + u, 0)
         return 0
 
     def b_all(i, _):
         step_b(n_seen + 2 * n_two + i, 0)
-        return score_all(seen_p + i, 0)
-
-    lax.fori_loop(0, n_two, sides_b, 0)
-    lax.fori_loop(2 * n_two, seen_p, score_sides, 0)
-    wait_queries(across)
-    lax.fori_loop(0, seen_p, score_across, 0)
+        return all_of(seen_p + i, 0)
+
+    lax.fori_loop(0, n_two, rest_b, 0)
+    lax.fori_loop(2 * n_two, seen_p, rest_of, 0)
     lax.fori_loop(0, max(rest, 0), b_all, 0)
-    lax.fori_loop(seen_p + max(rest, 0), pairs, score_all, 0)
-
-    part = min(512, keys_all)
-
-    def weigh(xp):
-        peak = jnp.max(mst[xp], axis=0, keepdims=True)
+    lax.fori_loop(seen_p + max(rest, 0), pairs, all_of, 0)
+
+    part = min(1024, keys_all)
+
+    def weigh(dx):
+        peak = jnp.max(mst[dx], axis=0, keepdims=True)
         l8 = jnp.zeros((8, 2 * ht), F32)
         o = jnp.zeros((128, 2 * ht), F32)
         for k in range(keys_all // part):
-            p = jnp.exp2(sco[xp, k * part : (k + 1) * part, :] - peak)
+            p = jnp.exp2(sco[dx, k * part : (k + 1) * part, :] - peak)
             l8 = l8 + jnp.sum(p.reshape(part // 8, 8, 2 * ht), axis=0)
             o = o + mm(latt[:, k * part : (k + 1) * part], p.astype(BF16))
         l = jnp.sum(l8, axis=0, keepdims=True)
-        pos[xp] = (o / l).astype(BF16)
-        pls[xp] = jnp.broadcast_to(peak + jnp.log(l) * LOG2E, (8, 2 * ht))
-
-    def weigh_next(i, _):
-        dx = i + 1
-        if nx == 4:
-            dx = jnp.where(dx == 3, 3, 3 - dx)
-        xo = lax.rem(x + dx, nx)
-        weigh(xo)
-        rc(pls.at[xo], plr.at[x], lss.at[i], lrs.at[x], s, xo * 2 + c).start()
-        rc(pos.at[xo], por.at[x], pss.at[i], prs.at[x], s, xo * 2 + c).start()
-        return 0
-
-    lax.fori_loop(0, nx - 1, weigh_next, 0)
-    weigh(x)
-    por[pl.ds(x, 1)] = pos[pl.ds(x, 1)]
-    plr[pl.ds(x, 1)] = pls[pl.ds(x, 1)]
+        return (o / l).astype(BF16), jnp.broadcast_to(peak + jnp.log(l) * LOG2E, (8, 2 * ht))
+
+    for i, dx in enumerate(across + sides):
+        pos[dx], pls[dx] = weigh(dx)
+        xo, back = lax.rem(x + dx, nx), nx - dx
+        rc(pls.at[dx], plr.at[back], lss.at[i], lrs.at[back], s, xo * 2 + c).start()
+        rc(pos.at[dx], por.at[back], pss.at[i], prs.at[back], s, xo * 2 + c).start()
+    por[0], plr[0] = weigh(0)
     for copy in local[early + 8 :]:
         copy.wait()
     for i in range(5, 8):
         done(wdone[i], wrsem.at[i])
     for dx in range(1, nx):
-        xo = lax.rem(x + dx, nx)
-        done(plr.at[xo], lrs.at[xo])
-        done(por.at[xo], prs.at[xo])
+        done(plr.at[dx], lrs.at[dx])
+        done(por.at[dx], prs.at[dx])
     lse = [plr[xp, 0:1, :] for xp in range(nx)]
     top = functools.reduce(jnp.maximum, lse)
     wts = [jnp.exp2(v - top) for v in lse]
@@ -549,27 +540,26 @@
     v = pltpu.VMEM
     scratch = [
         v((tok, ft), BF16), v((tp, ft), F32), v((1, 128), F32), v((sp, 128), F32),
-        v((tok, 128), F32), v((2, 8, 256), F32), v((2, model, 128), BF16),
+        v((tok, 128), F32), pltpu.SMEM((2,), F32), v((2, 8, 256), F32), v((2, model, 128), BF16),
         v((2, 320, model), BF16), v((ft, 128), BF16), v((64, ft), BF16),
         v((2, 128, 128), BF16), v((2, 128, 128), BF16), v((512, model), BF16),
         v((tp, sl, 256), BF16), v((tp, sl, 256), BF16), v((tp, ht, ft), BF16),
         v((2, ht, 128), F32), v((2, ht, 320), F32), v((ht, 1), F32),
         v((nz, 2, ny, sl + sl // 2, 128), BF16), v((nx, 192, 2 * ht), BF16),
         v((3, 2, ht, 128), BF16), v((512, ht), BF16), v((ht, 512), BF16),
-        v((nx, tok * sp // nx, 2 * ht), F32), v((128, tok * sp // nx), BF16),
-        v((tok * sp // nx, 192), BF16),
+        v((nx, tok * sp // nx, 2 * ht), F32),
+        v((128, tok * sp // nx), BF16), v((tok * sp // nx, 192), BF16),
         v((nx, 8, 2 * ht), F32),
         v((nx, 128, 2 * ht), BF16), v((nx, 128, 2 * ht), BF16),
         v((nx, 8, 2 * ht), F32), v((nx, 8, 2 * ht), F32),
         v((tp, ht, ft), BF16), v((nx, 2, ht, ft), BF16),
-        dma((14 + tp,)), dma((9,)), dma((9,)), dma((tp,)), dma((tp,)), dma((tp,)), dma((tp,)),
+        dma((15 + tp,)), dma((9,)), dma((9,)), dma((tp,)), dma((tp,)), dma((tp,)), dma((tp,)),
         dma((n_z,)), dma((nz,)), dma((nz, max(ny - 1, 1))), dma((nz,)), dma((nz,)), dma((nz,)),
         dma((nx,)), dma((nx,)), dma((2,)), dma((3,)), dma((nx,)), dma((nx,)), dma((nx,)), dma((nx,)),
         dma((tp,)), dma((nx, 2)),
     ]
     hbm = pl.BlockSpec(memory_space=pl.ANY)
     specs = [hbm] * 16
-    specs[5] = pl.BlockSpec(memory_space=pltpu.SMEM)
     return pl.pallas_call(
         functools.partial(kernel, cfg),
         out_shape=jax.ShapeDtypeStruct((tok, ft), BF16),

time: 59 us -> 58 us (0.983)
  Pallas kernels: 57.2 us -> 56.3 us
    pallas_call x1, Pallas kernels: 57.2 us -> 56.3 us  [per_device(): pl.pallas_call(functools.partial(kernel, cfg), out_shape=jax.ShapeDtypeSt...]
where the time goes in v4:
time: 58 us; the launch traced here: 57.9 us
  Pallas kernels  56.3 us (97%)
  local copies, waits for them, and re-layouts  1.57 us (3%)
    pallas_call x1, Pallas kernels, per_device(): pl.pallas_call(functools.partial(kernel, cfg), out_shape=jax.ShapeDtypeSt...  56.3 us
    unnamed x1, local copies, waits for them, and re-layouts  1.57 us

profile of v4, /device:TPU:1, one launch (start us, length us, event | category | flops | bytes accessed | tf_op | source)
XLA Modules:
  0.0 57.9 jit_solution(1892917865950459310)
XLA Ops:
  0.0 56.3 %shard_map.154 = bf16[256,256]{1,0:T(8,128)(2,1)} custom-call(bf16[256,256]{1,0:T(8,128)(2,1)} %act.1, f32[2048]{0:T(1024)} %gain.1, bf16[2048,128]{1,0:T(8,128)(2,1)} %wq.1, bf16[64,2048]{1,0:T(8,128)(2,1)} %bitcast.6, bf16[64,2048]{1,0:T(8,128)(2,1)} %bitcast.7, f32[2]{0:T(128)} %sink.1, bf16[192,2048]{1,0:T(8,128)(2,1)} %bitcast.5, ...), custom_call_target="tpu_custom_call" | custom-call | tf_op jit(solution)/shard_map/pallas_call | solution.py:563
  56.3 1.6 %copy.18 = bf16[256,256]{1,0:T(8,128)(2,1)} copy(bf16[256,256]{1,0:T(8,128)(2,1)} %shard_map.154) | data formatting | bytes 262144

commit v5 on v4

--- a/solution.py
+++ b/solution.py
@@ -36,7 +36,7 @@
         for k in range(1, REACH):
             near += [k, -k]
         rest = nz // 2 - REACH
-        return near, list(range(1, rest + 1))[::-1], [-k for k in range(1, rest)][::-1]
+        return near, list(range(1, rest + 1)), [-k for k in range(1, rest)]
     half = nz // 2
     near = []
     for k in range(1, half + 1):
@@ -57,7 +57,7 @@
     act, gain, wq, wk, wv, sink, wlq, wkvd, wrope, lgain, kup, vup, ow, ol, ta, tb,
     out,
     actv, gv, lgv, tav, tbv, sinkm, sinkv, wqv, wtv, kdv, krv, kupv, vupv, wall,
-    kps, kpr, xb, accq, acct, sqv,
+    kps, kpr, xb, accq, accl, sqv,
     kbuf, qt, kvb, catt, cat, sco, latt, keyb, mst, pos, por, pls, plr, rss, rsr,
     lsem, wssem, wrsem, kpssem, kprsem, xssem, xrsem, kzs, kzr, kys, kyr, kds, kdr,
     qss, qrs, hss, hrs, pss, prs, lss, lrs, rs_s, rs_r,
@@ -257,10 +257,9 @@
         xk = (xf * gv[pl.ds(k, 1), :]).astype(BF16)
         kr = pl.ds(pl.multiple_of(k * ft, ft), ft)
         for c2 in range(2):
-            term = mm(xk, wqv[c2, kr, :])
-            accq[c2] = term if first else accq[c2] + term
-            term = mm(xk, wtv[c2, :, kr], NT)
-            acct[c2] = term if first else acct[c2] + term
+            term = mm(xk, wtv[c2, 128:320, kr], NT)
+            accl[c2] = term if first else accl[c2] + term
+        xb[k] = xk
         sqv[...] = sq if first else sqv[...] + sq
 
     own_half = pl.ds(pl.multiple_of(c * ht, ht), ht)
@@ -298,7 +297,7 @@
     qcos, qsin = angles(c * ht, ht)
     factor = (PLAIN + D_ROPE) ** (-0.5) * LOG2E
     for c2 in range(2):
-        ql = acct[c2, :, 128:320] * scale
+        ql = accl[c2] * scale
         plain = ql[:, :PLAIN].astype(BF16)
         qt[0, 0:128, c2 * ht : (c2 + 1) * ht] = (mm(kupv[c2], plain, NT) * factor).astype(BF16)
         turned = rotate(ql[:, PLAIN:], qcos, qsin) * factor
@@ -310,11 +309,14 @@
         rc(qt.at[0], qt.at[nx - dx], qss.at[i], qrs.at[nx - dx], s, xo * 2 + c).start()
 
     for c2 in range(2):
-        kvb[1, c2] = (acct[c2, :, 0:128] * scale).astype(BF16)
-    to_mate = rc(kvb.at[1], kvb.at[2 * c], hss.at[0], hrs.at[2 * c], s, mate)
-    to_mate.start()
-    to_side = rc(kvb.at[1], kvb.at[2 * other], hss.at[1], hrs.at[2 * other], side, mate)
-    to_side.start()
+        kv = mm(xb[0], wtv[c2, 0:128, 0:ft], NT)
+        qw = mm(xb[0], wqv[c2, 0:ft, :])
+        for k in range(1, tp):
+            kr = slice(k * ft, (k + 1) * ft)
+            kv = kv + mm(xb[k], wtv[c2, 0:128, kr], NT)
+            qw = qw + mm(xb[k], wqv[c2, kr, :])
+        kvb[1, c2] = (kv * scale).astype(BF16)
+        accq[c2] = qw
 
     mst[...] = jnp.full(mst.shape, -jnp.inf, F32)
     nkeys = 2 * ny * sl
@@ -347,8 +349,13 @@
         score(i, 0)
         return 0
 
-    def rest_of(i, _):
-        for dx in across + sides:
+    def sides_of(i, _):
+        for dx in sides:
+            score(i, dx)
+        return 0
+
+    def across_of(i, _):
+        for dx in across:
             score(i, dx)
         return 0
 
@@ -364,13 +371,67 @@
 
     pairs = nz // 2
     seen_p = n_seen // 2
-    early_b, early_p, mid_p = min(5, n_seen), min(1, seen_p), min(2, seen_p)
-    lax.fori_loop(1, first_b, step_b, 0)
-    lax.fori_loop(0, early_p, prep, 0)
-    lax.fori_loop(first_b, early_b, step_b, 0)
-    lax.fori_loop(n_seen, nz, step_a, 0)
-    lax.fori_loop(early_b, n_seen, step_b, 0)
-    lax.fori_loop(early_p, mid_p, prep, 0)
+    cut = [min(n_seen + k, nz) for k in (0, 2, 4, 6)]
+    bs = [min(k, n_seen) for k in (3, 5, 7)]
+    p0, p1 = min(1, seen_p), min(2, seen_p)
+    lax.fori_loop(1, bs[0], step_b, 0)
+    lax.fori_loop(cut[0], cut[1], step_a, 0)
+    lax.fori_loop(0, p0, prep, 0)
+    lax.fori_loop(bs[0], bs[1], step_b, 0)
+    lax.fori_loop(cut[1], cut[2], step_a, 0)
+    lax.fori_loop(bs[1], bs[2], step_b, 0)
+    lax.fori_loop(cut[2], cut[3], step_a, 0)
+    lax.fori_loop(p0, p1, prep, 0)
+
+    lax.fori_loop(cut[3], nz, step_a, 0)
+    to_mate = rc(kvb.at[1], kvb.at[2 * c], hss.at[0], hrs.at[2 * c], s, mate)
+    to_mate.start()
+    to_side = rc(kvb.at[1], kvb.at[2 * other], hss.at[1], hrs.at[2 * other], side, mate)
+    to_side.start()
+    lax.fori_loop(bs[2], n_seen, step_b, 0)
+    lax.fori_loop(p1, seen_p, prep, 0)
+    wait_queries(sides)
+    n_two = seen_p // 2
+    rest = nz - n_seen - 2 * n_two
+
+    def rest_b(i, _):
+        for u in range(2):
+            sides_of(2 * i + u, 0)
+        for u in range(2 if rest >= 0 else 0):
+            step_b(n_seen + 2 * i + u, 0)
+        return 0
+
+    def b_all(i, _):
+        step_b(n_seen + 2 * n_two + i, 0)
+        return all_of(seen_p + i, 0)
+
+    lax.fori_loop(0, n_two, rest_b, 0)
+    lax.fori_loop(2 * n_two, seen_p, sides_of, 0)
+    wait_queries(across)
+    for i in range(seen_p):
+        across_of(i, 0)
+    lax.fori_loop(0, max(rest, 0), b_all, 0)
+    lax.fori_loop(seen_p + max(rest, 0), pairs, all_of, 0)
+
+    part = min(1024, keys_all)
+
+    def weigh(dx):
+        peak = jnp.max(mst[dx], axis=0, keepdims=True)
+        l8 = jnp.zeros((8, 2 * ht), F32)
+        o = jnp.zeros((128, 2 * ht), F32)
+        for k in range(keys_all // part):
+            p = jnp.exp2(sco[dx, k * part : (k + 1) * part, :] - peak)
+            l8 = l8 + jnp.sum(p.reshape(part // 8, 8, 2 * ht), axis=0)
+            o = o + mm(latt[:, k * part : (k + 1) * part], p.astype(BF16))
+        l = jnp.sum(l8, axis=0, keepdims=True)
+        return (o / l).astype(BF16), jnp.broadcast_to(peak + jnp.log(l) * LOG2E, (8, 2 * ht))
+
+    for i, dx in enumerate(across + sides):
+        pos[dx], pls[dx] = weigh(dx)
+        xo, back = lax.rem(x + dx, nx), nx - dx
+        rc(pls.at[dx], plr.at[back], lss.at[i], lrs.at[back], s, xo * 2 + c).start()
+        rc(pos.at[dx], por.at[back], pss.at[i], prs.at[back], s, xo * 2 + c).start()
+    por[0], plr[0] = weigh(0)
 
     for i in (0, 2):
         done(kvb.at[i], hrs.at[i])
@@ -399,46 +460,6 @@
             o = mm(vw, w.astype(BF16), TN) / den
             catt[(c2 * 2 + g) * DH : (c2 * 2 + g + 1) * DH, :] = o.astype(BF16)
 
-    lax.fori_loop(mid_p, seen_p, prep, 0)
-    wait_queries(sides + across)
-    n_two = seen_p // 2
-    rest = nz - n_seen - 2 * n_two
-
-    def rest_b(i, _):
-        for u in range(2):
-            rest_of(2 * i + u, 0)
-        for u in range(2 if rest >= 0 else 0):
-            step_b(n_seen + 2 * i + u, 0)
-        return 0
-
-    def b_all(i, _):
-        step_b(n_seen + 2 * n_two + i, 0)
-        return all_of(seen_p + i, 0)
-
-    lax.fori_loop(0, n_two, rest_b, 0)
-    lax.fori_loop(2 * n_two, seen_p, rest_of, 0)
-    lax.fori_loop(0, max(rest, 0), b_all, 0)
-    lax.fori_loop(seen_p + max(rest, 0), pairs, all_of, 0)
-
-    part = min(1024, keys_all)
-
-    def weigh(dx):
-        peak = jnp.max(mst[dx], axis=0, keepdims=True)
-        l8 = jnp.zeros((8, 2 * ht), F32)
-        o = jnp.zeros((128, 2 * ht), F32)
-        for k in range(keys_all // part):
-            p = jnp.exp2(sco[dx, k * part : (k + 1) * part, :] - peak)
-            l8 = l8 + jnp.sum(p.reshape(part // 8, 8, 2 * ht), axis=0)
-            o = o + mm(latt[:, k * part : (k + 1) * part], p.astype(BF16))
-        l = jnp.sum(l8, axis=0, keepdims=True)
-        return (o / l).astype(BF16), jnp.broadcast_to(peak + jnp.log(l) * LOG2E, (8, 2 * ht))
-
-    for i, dx in enumerate(across + sides):
-        pos[dx], pls[dx] = weigh(dx)
-        xo, back = lax.rem(x + dx, nx), nx - dx
-        rc(pls.at[dx], plr.at[back], lss.at[i], lrs.at[back], s, xo * 2 + c).start()
-        rc(pos.at[dx], por.at[back], pss.at[i], prs.at[back], s, xo * 2 + c).start()
-    por[0], plr[0] = weigh(0)
     for copy in local[early + 8 :]:
         copy.wait()
     for i in range(5, 8):
@@ -544,7 +565,7 @@
         v((2, 320, model), BF16), v((ft, 128), BF16), v((64, ft), BF16),
         v((2, 128, 128), BF16), v((2, 128, 128), BF16), v((512, model), BF16),
         v((tp, sl, 256), BF16), v((tp, sl, 256), BF16), v((tp, ht, ft), BF16),
-        v((2, ht, 128), F32), v((2, ht, 320), F32), v((ht, 1), F32),
+        v((2, ht, 128), F32), v((2, ht, 192), F32), v((ht, 1), F32),
         v((nz, 2, ny, sl + sl // 2, 128), BF16), v((nx, 192, 2 * ht), BF16),
         v((3, 2, ht, 128), BF16), v((512, ht), BF16), v((ht, 512), BF16),
         v((nx, tok * sp // nx, 2 * ht), F32),

time: 58 us -> 58.1 us (level)
  no operation moved by 1% of the time
where the time goes in v5:
time: 58.1 us; the launch traced here: 57.9 us
  Pallas kernels  56.3 us (97%)
  local copies, waits for them, and re-layouts  1.57 us (3%)
    pallas_call x1, Pallas kernels, per_device(): pl.pallas_call(functools.partial(kernel, cfg), out_shape=jax.ShapeDtypeSt...  56.3 us
    unnamed x1, local copies, waits for them, and re-layouts  1.57 us

profile of v5, /device:TPU:1, one launch (start us, length us, event | category | flops | bytes accessed | tf_op | source)
XLA Modules:
  0.0 57.9 jit_solution(5384837839908119134)
XLA Ops:
  0.0 56.3 %shard_map.154 = bf16[256,256]{1,0:T(8,128)(2,1)} custom-call(bf16[256,256]{1,0:T(8,128)(2,1)} %act.1, f32[2048]{0:T(1024)} %gain.1, bf16[2048,128]{1,0:T(8,128)(2,1)} %wq.1, bf16[64,2048]{1,0:T(8,128)(2,1)} %bitcast.6, bf16[64,2048]{1,0:T(8,128)(2,1)} %bitcast.7, f32[2]{0:T(128)} %sink.1, bf16[192,2048]{1,0:T(8,128)(2,1)} %bitcast.5, ...), custom_call_target="tpu_custom_call" | custom-call | tf_op jit(solution)/shard_map/pallas_call | solution.py:584
  56.4 1.6 %copy.18 = bf16[256,256]{1,0:T(8,128)(2,1)} copy(bf16[256,256]{1,0:T(8,128)(2,1)} %shard_map.154) | data formatting | bytes 262144

commit v6 on v5

--- a/solution.py
+++ b/solution.py
@@ -579,7 +579,8 @@
         dma((nx,)), dma((nx,)), dma((2,)), dma((3,)), dma((nx,)), dma((nx,)), dma((nx,)), dma((nx,)),
         dma((tp,)), dma((nx, 2)),
     ]
-    hbm = pl.BlockSpec(memory_space=pl.ANY)
+    keep = lambda a: pltpu.with_memory_space_constraint(a, pltpu.HBM)
+    hbm = pl.BlockSpec(memory_space=pltpu.HBM)
     specs = [hbm] * 16
     return pl.pallas_call(
         functools.partial(kernel, cfg),
@@ -588,10 +589,16 @@
         out_specs=pl.BlockSpec(memory_space=pltpu.VMEM),
         scratch_shapes=scratch,
         compiler_params=pltpu.CompilerParams(
-            collective_id=0, has_side_effects=True, vmem_limit_bytes=67043328
+            collective_id=0, has_side_effects=True, vmem_limit_bytes=44000 * 1024
         ),
     )(
-        act, gain, wq, wk.T, wv.T, sink, wlq.T, wkvd, wrope.T, lgain.reshape(1, 128), kup, vup, ow, ol, jnp.asarray(ta), jnp.asarray(tb),
+        *map(
+            keep,
+            (
+                act, gain, wq, wk.T, wv.T, sink, wlq.T, wkvd, wrope.T, lgain.reshape(1, 128),
+                kup, vup, ow, ol, jnp.asarray(ta), jnp.asarray(tb),
+            ),
+        )
     )
 
 

time: 58.1 us -> 56.5 us (0.972)
  local copies, waits for them, and re-layouts: 1.57 us -> 0.66 us
  Pallas kernels: 56.3 us -> 55.7 us
    unnamed x1, local copies, waits for them, and re-layouts: 1.57 us -> 0.66 us
    pallas_call x1, Pallas kernels: 56.3 us -> 55.7 us  [per_device(): pl.pallas_call(functools.partial(kernel, cfg), out_shape=jax.ShapeDtypeSt...]
where the time goes in v6:
time: 56.5 us; the launch traced here: 56.4 us
  Pallas kernels  55.7 us (99%)
  local copies, waits for them, and re-layouts  0.66 us (1%)
    pallas_call x1, Pallas kernels, per_device(): pl.pallas_call(functools.partial(kernel, cfg), out_shape=jax.ShapeDtypeSt...  55.7 us

profile of v6, /device:TPU:1, one launch (start us, length us, event | category | flops | bytes accessed | tf_op | source)
XLA Modules:
  0.0 56.4 jit_solution(13988385310048859195)
XLA Ops:
  0.0 55.7 %shard_map.154 = bf16[256,256]{1,0:T(8,128)(2,1)S(1)} custom-call(bf16[256,256]{1,0:T(8,128)(2,1)} %act.1, f32[2048]{0:T(1024)} %gain.1, bf16[2048,128]{1,0:T(8,128)(2,1)} %wq.1, bf16[64,2048]{1,0:T(8,128)(2,1)} %bitcast.6, bf16[64,2048]{1,0:T(8,128)(2,1)} %bitcast.7, f32[2]{0:T(128)} %sink.1, bf16[192,2048]{1,0:T(8,128)(2,1)} %bitcast.5, ...), custom_call_target="tpu_custom_call" | custom-call | tf_op jit(solution)/shard_map/pallas_call | solution.py:585
  55.7 0.7 %copy.18 = bf16[256,256]{1,0:T(8,128)(2,1)} copy(bf16[256,256]{1,0:T(8,128)(2,1)S(1)} %shard_map.154) | data formatting | bytes 262144

commit v7 on v6

--- a/solution.py
+++ b/solution.py
@@ -102,11 +102,11 @@
     def greet(sp_id, tp_id):
         pl.semaphore_signal(barrier, inc=1, device_id=(sp_id, tp_id), device_id_type=MESH)
 
+    for dz in near:
+        greet(at_z(dz) * ny + y, t)
+        n_sig += 1
     for d in range(1, tp):
         greet(s, lax.rem(t + d, tp))
-        n_sig += 1
-    for dz in near:
-        greet(at_z(dz) * ny + y, t)
         n_sig += 1
     for dy in range(1, ny):
         greet(z * ny + at_y(dy), t)

time: 56.5 us -> 56.5 us (level)
  no operation moved by 1% of the time
where the time goes in v7:
time: 56.5 us; the launch traced here: 56.3 us
  Pallas kernels  55.7 us (99%)
  local copies, waits for them, and re-layouts  0.66 us (1%)
    pallas_call x1, Pallas kernels, per_device(): pl.pallas_call(functools.partial(kernel, cfg), out_shape=jax.ShapeDtypeSt...  55.7 us

profile of v7, /device:TPU:1, one launch (start us, length us, event | category | flops | bytes accessed | tf_op | source)
XLA Modules:
  0.0 56.3 jit_solution(6627146004389821623)
XLA Ops:
  0.0 55.7 %shard_map.154 = bf16[256,256]{1,0:T(8,128)(2,1)S(1)} custom-call(bf16[256,256]{1,0:T(8,128)(2,1)} %act.1, f32[2048]{0:T(1024)} %gain.1, bf16[2048,128]{1,0:T(8,128)(2,1)} %wq.1, bf16[64,2048]{1,0:T(8,128)(2,1)} %bitcast.6, bf16[64,2048]{1,0:T(8,128)(2,1)} %bitcast.7, f32[2]{0:T(128)} %sink.1, bf16[192,2048]{1,0:T(8,128)(2,1)} %bitcast.5, ...), custom_call_target="tpu_custom_call" | custom-call | tf_op jit(solution)/shard_map/pallas_call | solution.py:585
  55.7 0.7 %copy.18 = bf16[256,256]{1,0:T(8,128)(2,1)} copy(bf16[256,256]{1,0:T(8,128)(2,1)S(1)} %shard_map.154) | data formatting | bytes 262144
